TPU v7x, 32 devices: a whole 2x2x4 slice. The times are simulated.
32 devices in a mesh: ep: 8 (over z, y), tp: 4 (over x, core).
Axes of the slice: x: 2, y: 2, z: 4, core: 2. Of those that a mesh axis runs over, the one named last changes fastest.
Arguments:
- query_latent: bfloat16 [1024, 768], P('ep'), may hold values from -6 to 6
- keyval_latent: bfloat16 [1024, 512], P('ep'), may hold values from -6 to 6
- rotary_key: bfloat16 [1024, 32], P('ep'), may hold values from -6 to 6
- query_gain: float32 [768], replicated, may hold values from 0.3 to 48
- keyval_gain: float32 [512], replicated, may hold values from 0.1 to 1.9
- query_weight: bfloat16 [768, 1536], P(None, 'tp'), may hold values from -0.21875 to 0.21875
- keyval_weight: bfloat16 [512, 2048], P(None, 'tp'), may hold values from -0.25 to 0.25
- output_weight: bfloat16 [1024, 2048], P('tp'), may hold values from -0.1875 to 0.1875
- output_gain: float32 [2048], replicated, may hold values from 0.1 to 1.9
- second_rows: bfloat16 [1024, 2048], P('ep'), may hold values from -6 to 6
- second_gain: float32 [2048], replicated, may hold values from 0.1 to 1.9
- route_ids: int32 [1024, 4], P('ep'), may hold values from 0 to 7, all different within a row; in each aligned block of 128 rows (0 to 127, 128 to 255, ...) at most 128 rows name the same one
- route_weights: float32 [1024, 4], P('ep'), may hold values from 0.1 to 1
- gate_weight: bfloat16 [8, 2048, 1024], P('ep', None, 'tp'), may hold values from -0.125 to 0.125
- up_weight: bfloat16 [8, 2048, 1024], P('ep', None, 'tp'), may hold values from -0.125 to 0.125
- down_weight: bfloat16 [8, 1024, 2048], P('ep', 'tp'), may hold values from -0.1875 to 0.1875
- shared_gate: bfloat16 [2048, 512], P(None, 'tp'), may hold values from -0.125 to 0.125
- shared_up: bfloat16 [2048, 512], P(None, 'tp'), may hold values from -0.125 to 0.125
- shared_down: bfloat16 [512, 2048], P('tp'), may hold values from -0.25 to 0.25
Outputs:
- mixed: bfloat16 [1024, 2048], P(('ep', 'tp'))
- expert_mix: bfloat16 [1024, 2048], P('ep', 'tp')
Inputs may be any that keep to these rules, and one draw needn't show every extreme that they name: `route_ids`: each row names 4 different experts. Among the rows of one index of ep (aligned blocks of 128 rows) no expert is named more than 128 times, a bound that some expert reaches in some blocks.
All inputs are finite; a program needn't handle non-finite values.
Results may differ from a plain program's by a relative error of at most 0.023.
The roundings to bfloat16 on the way count: a program that leaves them out, or rounds other values in their place, can miss the bound.
Values may be sent and summed in bfloat16 or wider, within the bound.
A program may use at most 128 MiB of HBM per device.

v0:
```python
import functools
import math

import jax
import jax.numpy as jnp
from jax import lax
from jax.experimental import pallas as pl
from jax.experimental.pallas import tpu as pltpu
from jax.sharding import PartitionSpec as P

NOPE = 64
ROPE = 32
VDIM = 64


EPS = 1e-06
ROPE_BASE = 10000.0


def rms_scale(values, gain_vec):
    widened = values.astype(jnp.float32)
    normed = widened * lax.rsqrt(jnp.mean(widened * widened, -1, keepdims=True) + EPS)
    return (normed * gain_vec).astype(jnp.bfloat16)


def rotate(values, positions):
    half_width = values.shape[-1] // 2
    inverse = 1.0 / ROPE_BASE ** (
        jnp.arange(half_width, dtype=jnp.float32) * 2.0 / (2 * half_width)
    )
    angles = positions[:, None] * inverse[None, :]
    cosine = jnp.cos(angles)
    sine_vals = jnp.sin(angles)
    if values.ndim == 3:
        cosine = cosine[:, None, :]
        sine_vals = sine_vals[:, None, :]
    first_half = values[..., :half_width]
    second = values[..., half_width:]
    return jnp.concatenate(
        [first_half * cosine - second * sine_vals, first_half * sine_vals + second * cosine], -1
    )


def per_device_slots(
    query_latent,
    keyval_latent,
    rotary_key,
    query_gain,
    keyval_gain,
    query_weight,
    keyval_weight,
    output_weight,
    output_gain,
    second_rows,
    second_gain,
    route_ids,
    route_weights,
    gate_weight,
    up_weight,
    down_weight,
    shared_gate,
    shared_up,
    shared_down,
):
    first_rows = query_latent.shape[0]
    tp_count = lax.axis_size("tp")
    ep_count = lax.axis_size("ep")
    head_count = query_weight.shape[1] // (NOPE + ROPE)
    positions = (lax.axis_index("ep") * first_rows).astype(jnp.float32) + jnp.arange(
        first_rows, dtype=jnp.float32
    )
    queries = jnp.dot(
        rms_scale(query_latent, query_gain), query_weight, preferred_element_type=jnp.float32
    ).reshape(first_rows, head_count, NOPE + ROPE)
    queries = jnp.concatenate(
        [queries[..., :NOPE], rotate(queries[..., NOPE:], positions)], -1
    ).astype(jnp.bfloat16)
    query_plain = queries[..., :NOPE]
    query_turned = queries[..., NOPE:]
    kv_normed = rms_scale(keyval_latent, keyval_gain)
    key_rot = rotate(rotary_key.astype(jnp.float32), positions).astype(jnp.bfloat16)
    score_scale = (NOPE + ROPE) ** (-0.5)

    def attend(carried, pieces):
        highest, denominator, accumulated = carried
        keyval_piece, rot_piece = pieces
        key_count = keyval_piece.shape[0]
        keyval_heads = keyval_piece.reshape(key_count, head_count, NOPE + VDIM)
        scores = jnp.einsum(
            "qhd,khd->hqk",
            query_plain,
            keyval_heads[..., :NOPE],
            preferred_element_type=jnp.float32,
        )
        scores = (
            scores
            + jnp.einsum("qhr,kr->hqk", query_turned, rot_piece, preferred_element_type=jnp.float32)
        ) * score_scale
        new_high = jnp.maximum(highest, jnp.max(scores, -1))
        exponent = jnp.exp(scores - new_high[..., None])
        rescale = jnp.exp(highest - new_high)
        denominator = denominator * rescale + jnp.sum(exponent, -1)
        update = jnp.einsum(
            "hqk,khe->qhe",
            exponent.astype(jnp.bfloat16),
            keyval_heads[..., NOPE:],
            preferred_element_type=jnp.float32,
        )
        accumulated = accumulated * rescale.T[..., None] + update
        return (new_high, denominator, accumulated)

    start_state = (
        jnp.full((head_count, first_rows), -jnp.inf, jnp.float32),
        jnp.zeros((head_count, first_rows), jnp.float32),
        jnp.zeros((first_rows, head_count, VDIM), jnp.float32),
    )
    quarter = first_rows // tp_count
    offset = lax.axis_index("tp") * quarter
    own_latent = lax.dynamic_slice_in_dim(kv_normed, offset, quarter, 0)
    own_rot = lax.dynamic_slice_in_dim(key_rot, offset, quarter, 0)
    all_latent, all_rot = (
        lax.all_gather(own_latent, ("ep", "tp"), axis=0, tiled=True),
        lax.all_gather(own_rot, ("ep", "tp"), axis=0, tiled=True),
    )
    total_keys = all_latent.shape[0]
    key_block = math.gcd(total_keys, 512)
    latent_blocks = all_latent.reshape(total_keys // key_block, key_block, all_latent.shape[1])
    rot_blocks = all_rot.reshape(total_keys // key_block, key_block, all_rot.shape[1])

    def scan_step(carried, block_pair):
        projected = jnp.dot(
            block_pair[0], keyval_weight, preferred_element_type=jnp.float32
        ).astype(jnp.bfloat16)
        return (attend(carried, (projected, block_pair[1])), None)

    final_state, _ = lax.scan(scan_step, start_state, (latent_blocks, rot_blocks))
    denominator = final_state[1]
    accumulated = final_state[2]
    attended = (
        (accumulated / denominator.T[..., None])
        .astype(jnp.bfloat16)
        .reshape(first_rows, head_count * VDIM)
    )
    mixture = lax.psum_scatter(
        jnp.dot(attended, output_weight, preferred_element_type=jnp.float32).astype(jnp.bfloat16),
        "tp",
        scatter_dimension=0,
        tiled=True,
    ).astype(jnp.float32)
    mixed = rms_scale(mixture, output_gain)
    tok_rows = second_rows.shape[0]
    model_width = second_rows.shape[1]
    top_count = route_ids.shape[1]
    local_count = gate_weight.shape[0]
    expert_count = local_count * ep_count
    capacity = max(tp_count, tok_rows * top_count * 2 // expert_count // tp_count * tp_count)
    normed = rms_scale(second_rows, second_gain)
    flat_ids = route_ids.reshape(-1)
    onehot = (flat_ids[:, None] == jnp.arange(expert_count, dtype=jnp.int32)[None, :]).astype(
        jnp.int32
    )
    slot_rank = jnp.sum((jnp.cumsum(onehot, 0) - 1) * onehot, 1)
    owners = jnp.arange(tok_rows * top_count, dtype=jnp.int32) // top_count
    slot_table = (
        jnp.full((expert_count * capacity,), tok_rows, jnp.int32)
        .at[flat_ids * capacity + slot_rank]
        .set(owners)
    )
    padded = jnp.concatenate([normed, jnp.zeros((1, model_width), jnp.bfloat16)], 0)
    outgoing = padded[slot_table].reshape(ep_count, local_count, capacity, model_width)
    weights = route_weights.reshape(-1, 1)
    shared_hidden = (
        jax.nn.silu(jnp.dot(normed, shared_gate, preferred_element_type=jnp.float32))
        * jnp.dot(normed, shared_up, preferred_element_type=jnp.float32)
    ).astype(jnp.bfloat16)
    shared_part = jnp.dot(shared_hidden, shared_down, preferred_element_type=jnp.float32)
    arrived = lax.all_to_all(outgoing, "ep", split_axis=0, concat_axis=0, tiled=True)
    gate_act = jnp.einsum(
        "sicd,idf->sicf", arrived, gate_weight, preferred_element_type=jnp.float32
    )
    up_act = jnp.einsum("sicd,idf->sicf", arrived, up_weight, preferred_element_type=jnp.float32)
    hidden = (jax.nn.silu(gate_act) * up_act).astype(jnp.bfloat16)
    slot_terms = jnp.einsum(
        "sicf,ifd->sicd", hidden, down_weight, preferred_element_type=jnp.float32
    ).reshape(-1, model_width)
    slot_sum, shared_sum = (
        lax.psum_scatter(
            slot_terms.astype(jnp.bfloat16), "tp", scatter_dimension=1, tiled=True
        ).astype(jnp.float32),
        lax.psum_scatter(
            shared_part.astype(jnp.bfloat16), "tp", scatter_dimension=1, tiled=True
        ).astype(jnp.float32),
    )
    column_part = model_width // tp_count
    returned = lax.all_to_all(
        slot_sum.astype(jnp.bfloat16).reshape(ep_count, local_count * capacity, column_part),
        "ep",
        split_axis=0,
        concat_axis=0,
        tiled=True,
    )
    returned = returned.reshape(expert_count * capacity, column_part)
    picked = returned[flat_ids * capacity + slot_rank].astype(jnp.float32) * weights
    routed = jnp.sum(picked.reshape(tok_rows, top_count, column_part), 1)
    expert_mix = (routed + shared_sum).astype(jnp.bfloat16)
    return (mixed, expert_mix)


MESH = pl.DeviceIdType.MESH


def grid_of(ep_count, tp_count):
    y_count = math.gcd(ep_count, 2)
    k_count = math.gcd(tp_count, 2)
    return (ep_count // y_count, y_count, tp_count // k_count, k_count)


def place_of(dims):
    ep_at, tp_at = lax.axis_index("ep"), lax.axis_index("tp")
    return (
        lax.div(ep_at, dims[1]),
        lax.rem(ep_at, dims[1]),
        lax.div(tp_at, dims[3]),
        lax.rem(tp_at, dims[3]),
    )


def moved(dims, place, dz=0, dy=0, dx=0, dk=0):
    return tuple(
        lax.rem(at + step % size, size) if step % size else at
        for at, step, size in zip(place, (dz, dy, dx, dk), dims)
    )


def device_of(dims, place):
    return (place[0] * dims[1] + place[1], place[2] * dims[3] + place[3])


def block_of(dims, place):
    ep_at, tp_at = device_of(dims, place)
    return ep_at * (dims[2] * dims[3]) + tp_at


def peers_of(dims):
    axes = ("dz", "dy", "dx", "dk")
    return [{axis: step} for axis, size in zip(axes, dims) for step in range(1, size)]


def meet(dims, place):
    barrier = pltpu.get_barrier_semaphore()
    peers = peers_of(dims)
    for peer in peers:
        pl.semaphore_signal(
            barrier,
            inc=1,
            device_id=device_of(dims, moved(dims, place, **peer)),
            device_id_type=MESH,
        )
    pl.semaphore_wait(barrier, len(peers))


def far_first(size):
    return sorted(range(1, size), key=lambda step: -min(step, size - step))


def gather_keys(dims):
    z_count, y_count, x_count, k_count = dims
    keys = []
    for dz in range(z_count):
        keys += [("z", dz, 0, 0, 0)]
        keys += [("x", dz, 0, dx, 0) for dx in range(1, x_count)]
        keys += [("y", dz, dy, 0, 0) for dy in range(1, y_count)]
        for dy in range(y_count):
            for dx in range(x_count):
                if dx and dy:
                    keys += [("p", dz, dy, dx, 0), ("q", dz, dy, dx, 0)]
                keys += [("k", dz, dy, dx, dk) for dk in range(1, k_count)]
    return {key: index for index, key in enumerate(keys)}


def gather_kernel(dims, *refs):
    count = (len(refs) - 2) // 2
    owns, alls, (send_sem, recv_sem) = refs[:count], refs[count : 2 * count], refs[2 * count :]
    keys = gather_keys(dims)
    z_count, y_count, x_count, k_count = dims
    me = place_of(dims)
    meet(dims, me)
    sent = []

    def region(which, place, half):
        rows = owns[which].shape[0]
        begin = pl.multiple_of(block_of(dims, place) * rows, rows)
        if half is None:
            return alls[which].at[pl.ds(begin, rows), :]
        return alls[which].at[pl.ds(begin + half * (rows // 2), rows // 2), :]

    def describe(which, key, source, place, half, target):
        return pltpu.make_async_remote_copy(
            src_ref=source,
            dst_ref=region(which, place, half),
            send_sem=send_sem.at[which, keys[key]],
            recv_sem=recv_sem.at[which, keys[key]],
            device_id=device_of(dims, target),
            device_id_type=MESH,
        )

    def send(which, key, origin, half, **step):
        source = region(which, origin, half)
        if origin is me:
            source = owns[which]
        copy = describe(which, key, source, origin, half, moved(dims, me, **step))
        copy.start()
        sent.append(copy)

    def arrive(which, key, origin, half=None):
        source = region(which, origin, half)
        describe(which, key, source, origin, half, me).wait_recv()

    def back(dz=0, dy=0, dx=0, dk=0):
        if not (dz or dy or dx or dk):
            return me
        return moved(dims, me, -dz, -dy, -dx, -dk)

    def to_partner(which, dz, dy, dx):
        for dk in range(1, k_count):
            send(which, ("k", dz, dy, dx, dk), back(dz, dy, dx), None, dk=dk)

    order = [0] + far_first(z_count)[::-1]
    for which in range(count):
        for dz in far_first(z_count):
            send(which, ("z", dz, 0, 0, 0), me, None, dz=dz)
    for which in range(count):
        for dz in order:
            if dz:
                arrive(which, ("z", dz, 0, 0, 0), back(dz))
            for dx in range(1, x_count):
                send(which, ("x", dz, 0, dx, 0), back(dz), None, dx=dx)
            for dy in range(1, y_count):
                send(which, ("y", dz, dy, 0, 0), back(dz), None, dy=dy)
            to_partner(which, dz, 0, 0)
    for which in range(count):
        alls[which][
            pl.ds(
                pl.multiple_of(block_of(dims, me) * owns[which].shape[0], owns[which].shape[0]),
                owns[which].shape[0],
            ),
            :,
        ] = owns[which][...]
    for which in range(count):
        for dz in order:
            for dx in range(1, x_count):
                arrive(which, ("x", dz, 0, dx, 0), back(dz, 0, dx))
                for dy in range(1, y_count):
                    send(which, ("p", dz, dy, dx, 0), back(dz, 0, dx), 0, dy=dy)
                to_partner(which, dz, 0, dx)
            for dy in range(1, y_count):
                arrive(which, ("y", dz, dy, 0, 0), back(dz, dy, 0))
                for dx in range(1, x_count):
                    send(which, ("q", dz, dy, dx, 0), back(dz, dy, 0), 1, dx=dx)
                to_partner(which, dz, dy, 0)
    for which in range(count):
        for dz in order:
            for dy in range(1, y_count):
                for dx in range(1, x_count):
                    arrive(which, ("p", dz, dy, dx, 0), back(dz, dy, dx), 0)
                    arrive(which, ("q", dz, dy, dx, 0), back(dz, dy, dx), 1)
                    to_partner(which, dz, dy, dx)
    for which in range(count):
        for dz in order:
            for dy in range(y_count):
                for dx in range(x_count):
                    for dk in range(1, k_count):
                        arrive(which, ("k", dz, dy, dx, dk), back(dz, dy, dx, dk))
    for copy in sent:
        copy.wait_send()


def gather_all(arrays, ep_count, tp_count):
    dims = grid_of(ep_count, tp_count)
    semaphores = (len(arrays), len(gather_keys(dims)))
    vmem = pl.BlockSpec(memory_space=pltpu.VMEM)
    return pl.pallas_call(
        functools.partial(gather_kernel, dims),
        out_shape=[
            jax.ShapeDtypeStruct((a.shape[0] * ep_count * tp_count, a.shape[1]), a.dtype)
            for a in arrays
        ],
        in_specs=[vmem] * len(arrays),
        out_specs=[vmem] * len(arrays),
        scratch_shapes=[pltpu.SemaphoreType.DMA(semaphores), pltpu.SemaphoreType.DMA(semaphores)],
        compiler_params=pltpu.CompilerParams(
            collective_id=0, has_side_effects=True, vmem_limit_bytes=32 * 1024 * 1024
        ),
    )(*arrays)


def reduce_keys(dims):
    z_count, y_count, x_count, k_count = dims
    keys = []
    for dz in range(z_count):
        for dy in range(y_count):
            for dx in range(x_count):
                keys += [("k", dz, dy, dx, dk) for dk in range(1, k_count)]
                if dx and dy:
                    keys += [("p", dz, dy, dx), ("q", dz, dy, dx)]
                elif dx:
                    keys += [("x", dz, dx)]
                elif dy:
                    keys += [("y", dz, dy)]
                elif dz:
                    keys += [("z", dz)]
    for dx in range(x_count):
        keys += [("mk", dx, dk) for dk in range(1, k_count)]
        if dx:
            keys += [("mx", dx)]
    return {key: index for index, key in enumerate(keys)}


def reduce_slots(dims):
    slots = {}
    for key in reduce_keys(dims):
        group = "pq" if key[0] in "pq" else ("m" if key[0][0] == "m" else "full")
        taken = sum(1 for other in slots.values() if other[0] == group)
        slots[key] = (group, taken)
    sizes = {
        group: max(1, sum(1 for other in slots.values() if other[0] == group))
        for group in ("pq", "m", "full")
    }
    return slots, sizes


def reduce_kernel(
    dims,
    rows_ref,
    scale_ref,
    gate_ref,
    up_ref,
    down_ref,
    shared_gate_ref,
    shared_up_ref,
    shared_down_ref,
    head_ref,
    gain_ref,
    mixed_ref,
    out_ref,
    parts_ref,
    full,
    halves,
    mixes,
    sums,
    mix_sums,
    send_sem,
    recv_sem,
):
    keys = reduce_keys(dims)
    slots, _ = reduce_slots(dims)
    stores = {"pq": halves, "m": mixes, "full": full}
    z_count, y_count, x_count, k_count = dims
    me = place_of(dims)
    rows = out_ref.shape[0]
    half_rows = rows // 2
    mix_rows = mixed_ref.shape[0]
    meet(dims, me)
    sent = []

    def landing(key):
        group, index = slots[key]
        return stores[group].at[index]

    def describe(key, source, target):
        return pltpu.make_async_remote_copy(
            src_ref=source,
            dst_ref=landing(key),
            send_sem=send_sem.at[keys[key]],
            recv_sem=recv_sem.at[keys[key]],
            device_id=device_of(dims, target),
            device_id_type=MESH,
        )

    def send(key, source, **step):
        copy = describe(key, source, moved(dims, me, **step))
        copy.start()
        sent.append(copy)

    def landed(key):
        describe(key, landing(key), me).wait_recv()
        return landing(key)[...].astype(jnp.float32)

    def part_of(dz, dy, dx, dk):
        column = device_of(dims, moved(dims, me, dx=dx, dk=dk))[1]
        return parts_ref.at[dz * y_count + dy, column]

    def compute(dz, dy):
        begin = device_of(dims, moved(dims, me, dz=dz, dy=dy))[0] * rows
        span = pl.ds(pl.multiple_of(begin, rows), rows)
        tokens = rows_ref[span, :]
        gate_act = jnp.dot(tokens, gate_ref[...], preferred_element_type=jnp.float32)
        up_act = jnp.dot(tokens, up_ref[...], preferred_element_type=jnp.float32)
        hidden = gate_act / (1.0 + jnp.exp(-gate_act)) * up_act * scale_ref[span, :]
        hidden = hidden.astype(jnp.bfloat16)
        own = dz == 0 and dy == 0
        if own:
            gate_own = jnp.dot(tokens, shared_gate_ref[...], preferred_element_type=jnp.float32)
            up_own = jnp.dot(tokens, shared_up_ref[...], preferred_element_type=jnp.float32)
            hidden_own = gate_own / (1.0 + jnp.exp(-gate_own)) * up_own
            hidden_own = hidden_own.astype(jnp.bfloat16)
        part = out_ref.shape[1]
        for column in range(x_count * k_count):
            columns = pl.ds(column * part, part)
            value = jnp.dot(hidden, down_ref[:, columns], preferred_element_type=jnp.float32)
            if own:
                value += jnp.dot(
                    hidden_own, shared_down_ref[:, columns], preferred_element_type=jnp.float32
                )
            parts_ref[dz * y_count + dy, column] = value.astype(jnp.bfloat16)
        for dx in range(x_count - 1, -1, -1):
            for dk in range(1, k_count):
                send(("k", dz, dy, dx, dk), part_of(dz, dy, dx, dk), dk=dk)

    def mix_span(dx, dk):
        begin = device_of(dims, moved(dims, me, dx=dx, dk=dk))[1] * mix_rows
        return pl.ds(pl.multiple_of(begin, mix_rows), mix_rows)

    z_steps = far_first(z_count) + [0]
    for dx in range(x_count):
        for dk in range(1, k_count):
            send(("mk", dx, dk), head_ref.at[mix_span(dx, dk)], dk=dk)

    def core_sum(place):
        value = part_of(*place, 0)[...].astype(jnp.float32)
        for dk in range(1, k_count):
            value = value + landed(("k", *place, dk))
        return value

    index_of = {}

    def keep(place, value):
        index_of[place] = len(index_of)
        sums[index_of[place]] = value.astype(jnp.bfloat16)
        return index_of[place]

    def mix_core(dx):
        value = head_ref[mix_span(dx, 0), :].astype(jnp.float32)
        for dk in range(1, k_count):
            value = value + landed(("mk", dx, dk))
        return value

    def finish(dz, dy):
        if dy:
            for dx in range(1, x_count):
                index = keep((dz, dy, dx), core_sum((dz, dy, dx)))
                send(("p", dz, dy, dx), sums.at[index, pl.ds(0, half_rows)], dy=dy)
                send(("q", dz, dy, dx), sums.at[index, pl.ds(half_rows, half_rows)], dx=dx)
            return
        for over in range(1, y_count):
            value = core_sum((dz, over, 0))
            upper, lower = value[:half_rows], value[half_rows:]
            for dx in range(1, x_count):
                lower = lower + landed(("q", dz, over, dx))
            index = keep((dz, over, 0), jnp.concatenate([upper, lower], 0))
            send(("y", dz, over), sums.at[index], dy=over)
        for dx in range(1, x_count):
            value = core_sum((dz, 0, dx))
            upper, lower = value[:half_rows], value[half_rows:]
            for over in range(1, y_count):
                upper = upper + landed(("p", dz, over, dx))
            index = keep((dz, 0, dx), jnp.concatenate([upper, lower], 0))
            send(("x", dz, dx), sums.at[index], dx=dx)

    blocks = [(dz, dy) for dy in list(range(1, y_count)) + [0] for dz in z_steps]
    for turn, block in enumerate(blocks):
        compute(*block)
        if turn:
            finish(*blocks[turn - 1])
        else:
            for dx in range(1, x_count):
                mix_sums[dx - 1] = mix_core(dx).astype(jnp.bfloat16)
                send(("mx", dx), mix_sums.at[dx - 1], dx=dx)
    finish(*blocks[-1])
    mixture = mix_core(0)
    for dx in range(1, x_count):
        mixture = mixture + landed(("mx", dx))
    scale = lax.rsqrt(jnp.mean(mixture * mixture, -1, keepdims=True) + EPS)
    mixed_ref[...] = (mixture * scale * gain_ref[...]).astype(jnp.bfloat16)
    for dz in z_steps:
        value = core_sum((dz, 0, 0))
        for dx in range(1, x_count):
            value = value + landed(("x", dz, dx))
        for dy in range(1, y_count):
            value = value + landed(("y", dz, dy))
        if dz:
            index = keep((dz, 0, 0), value)
            send(("z", dz), sums.at[index], dz=dz)
    for dz in range(1, z_count):
        value = value + landed(("z", dz))
    out_ref[...] = value.astype(jnp.bfloat16)
    for copy in sent:
        copy.wait_send()


def reduce_all(expert_args, head_part, gain, ep_count, tp_count):
    dims = grid_of(ep_count, tp_count)
    _, sizes = reduce_slots(dims)
    count, model_width = expert_args[0].shape
    rows = count // ep_count
    width = model_width // tp_count
    mix_rows = head_part.shape[0] // tp_count
    mix_width = head_part.shape[1]
    vmem = pl.BlockSpec(memory_space=pltpu.VMEM)
    semaphores = pltpu.SemaphoreType.DMA((len(reduce_keys(dims)),))
    return pl.pallas_call(
        functools.partial(reduce_kernel, dims),
        out_shape=[
            jax.ShapeDtypeStruct((mix_rows, mix_width), jnp.bfloat16),
            jax.ShapeDtypeStruct((rows, width), jnp.bfloat16),
        ],
        in_specs=[vmem] * (len(expert_args) + 2),
        out_specs=[vmem] * 2,
        scratch_shapes=[
            pltpu.VMEM((ep_count, tp_count, rows, width), jnp.bfloat16),
            pltpu.VMEM((sizes["full"], rows, width), jnp.bfloat16),
            pltpu.VMEM((sizes["pq"], rows // 2, width), jnp.bfloat16),
            pltpu.VMEM((sizes["m"], mix_rows, mix_width), jnp.bfloat16),
            pltpu.VMEM((dims[0] * dims[1] * dims[2], rows, width), jnp.bfloat16),
            pltpu.VMEM((max(1, dims[2] - 1), mix_rows, mix_width), jnp.bfloat16),
            semaphores,
            semaphores,
        ],
        compiler_params=pltpu.CompilerParams(
            collective_id=1, has_side_effects=True, vmem_limit_bytes=48 * 1024 * 1024
        ),
    )(*expert_args, head_part, gain)


def per_device_dense(
    query_latent,
    keyval_latent,
    rotary_key,
    query_gain,
    keyval_gain,
    query_weight,
    keyval_weight,
    output_weight,
    output_gain,
    second_rows,
    second_gain,
    route_ids,
    route_weights,
    gate_weight,
    up_weight,
    down_weight,
    shared_gate,
    shared_up,
    shared_down,
):
    first_rows = query_latent.shape[0]
    tp_count = lax.axis_size("tp")
    ep_count = lax.axis_size("ep")
    head_count = query_weight.shape[1] // (NOPE + ROPE)
    start_row = lax.axis_index("ep") * first_rows
    quarter = first_rows // tp_count
    offset = lax.axis_index("tp") * quarter
    second_quarter = second_rows.shape[0] // tp_count
    second_offset = lax.axis_index("tp") * second_quarter

    own_latent = rms_scale(
        lax.dynamic_slice_in_dim(keyval_latent, offset, quarter, 0), keyval_gain
    )
    own_positions = (start_row + offset).astype(jnp.float32) + jnp.arange(
        quarter, dtype=jnp.float32
    )
    own_rot = rotate(
        lax.dynamic_slice_in_dim(rotary_key, offset, quarter, 0).astype(jnp.float32),
        own_positions,
    ).astype(jnp.bfloat16)
    ids = lax.dynamic_slice_in_dim(route_ids, second_offset, second_quarter, 0)
    wts = lax.dynamic_slice_in_dim(route_weights, second_offset, second_quarter, 0)
    dense = jnp.sum(
        jnp.where(
            ids[:, :, None] == jnp.arange(ep_count, dtype=jnp.int32)[None, None, :],
            wts[:, :, None],
            0.0,
        ),
        1,
    )
    dense_high = dense.astype(jnp.bfloat16)
    dense_low = (dense - dense_high.astype(jnp.float32)).astype(jnp.bfloat16)
    latent_width = own_latent.shape[1]
    used = latent_width + ROPE + 2 * ep_count
    fill = -used % 128
    packed = jnp.concatenate(
        [own_latent, own_rot, dense_high, dense_low, jnp.zeros((quarter, fill), jnp.bfloat16)], 1
    )
    own_normed = rms_scale(
        lax.dynamic_slice_in_dim(second_rows, second_offset, second_quarter, 0), second_gain
    )
    packed, normed = gather_all([packed, own_normed], ep_count, tp_count)

    positions = start_row.astype(jnp.float32) + jnp.arange(first_rows, dtype=jnp.float32)
    queries = jnp.dot(
        rms_scale(query_latent, query_gain), query_weight, preferred_element_type=jnp.float32
    ).reshape(first_rows, head_count, NOPE + ROPE)
    queries = jnp.concatenate(
        [queries[..., :NOPE], rotate(queries[..., NOPE:], positions)], -1
    ).astype(jnp.bfloat16)
    all_latent = packed[:, :latent_width]
    all_rot = packed[:, latent_width : latent_width + ROPE]
    total_keys = packed.shape[0]
    keyvals = (
        jnp.dot(all_latent, keyval_weight, preferred_element_type=jnp.float32)
        .astype(jnp.bfloat16)
        .reshape(total_keys, head_count, NOPE + VDIM)
    )
    keys = jnp.concatenate(
        [
            keyvals[..., :NOPE],
            jnp.broadcast_to(all_rot[:, None, :], (total_keys, head_count, ROPE)),
        ],
        -1,
    )
    scores = jnp.einsum("qhd,khd->hqk", queries, keys, preferred_element_type=jnp.float32) * (
        (NOPE + ROPE) ** (-0.5)
    )
    exponent = jnp.exp(scores - jnp.max(scores, -1, keepdims=True))
    denominator = jnp.sum(exponent, -1)
    accumulated = jnp.einsum(
        "hqk,khe->qhe",
        exponent.astype(jnp.bfloat16),
        keyvals[..., NOPE:],
        preferred_element_type=jnp.float32,
    )
    attended = (
        (accumulated / denominator.T[..., None])
        .astype(jnp.bfloat16)
        .reshape(first_rows, head_count * VDIM)
    )
    head_part = jnp.dot(attended, output_weight, preferred_element_type=jnp.float32).astype(
        jnp.bfloat16
    )

    me = lax.axis_index("ep")
    high = lax.dynamic_slice_in_dim(packed, latent_width + ROPE + me, 1, 1)
    low = lax.dynamic_slice_in_dim(packed, latent_width + ROPE + ep_count + me, 1, 1)
    scale = high.astype(jnp.float32) + low.astype(jnp.float32)
    expert_args = (
        normed,
        scale,
        gate_weight[0],
        up_weight[0],
        down_weight[0],
        shared_gate,
        shared_up,
        shared_down,
    )
    mixed, expert_mix = reduce_all(
        expert_args, head_part, output_gain.reshape(1, -1), ep_count, tp_count
    )
    return (mixed, expert_mix)


def solution(mesh):
    placed = (
        P("ep", None),
        P("ep", None),
        P("ep", None),
        P(),
        P(),
        P(None, "tp"),
        P(None, "tp"),
        P("tp", None),
        P(),
        P("ep", None),
        P(),
        P("ep", None),
        P("ep", None),
        P("ep", None, "tp"),
        P("ep", None, "tp"),
        P("ep", "tp", None),
        P(None, "tp"),
        P(None, "tp"),
        P("tp", None),
    )
    def per_device(*args):
        tok_rows, top_count = args[11].shape
        expert_count = args[13].shape[0] * mesh.shape["ep"]
        capacity = tok_rows * top_count * 2 // expert_count
        if args[13].shape[0] == 1 and capacity >= tok_rows:
            return per_device_dense(*args)
        return per_device_slots(*args)

    return jax.shard_map(
        per_device,
        mesh=mesh,
        in_specs=placed,
        out_specs=(P(("ep", "tp"), None), P("ep", "tp")),
        check_vma=False,
    )
```

profile of v0, /device:TPU:0, one launch (start us, length us, event | category | flops | bytes accessed | tf_op | source)
XLA Modules:
  0.0 90.9 jit_solution(6616720258251912283)
XLA Ops:
  0.6 0.0 copy-start
  0.7 1.1 %fusion.13 = f32[128]{0:T(128)S(1)} fusion(bf16[128,768]{1,0:T(8,128)(2,1)} %param.19), kind=kLoop, calls=%fused_computation.20 | loop fusion | flops 294784 | bytes 197120 | tf_op jit(solution)/shard_map/reduce_sum | solution.py:22
  1.8 0.9 fusion.28
  2.7 1.0 %fusion.16 = f32[32]{0:T(128)S(1)} fusion(bf16[128,2048]{1,0:T(8,128)(2,1)} %param.28, s32[]{:T(128)S(6)} %select_n.17), kind=kLoop, calls=%fused_computation.25 | loop fusion | flops 196576 | bytes 131204 | tf_op jit(solution)/shard_map/reduce_sum | solution.py:22
  3.8 0.8 constant_dynamic-slice_fusion.1
  4.5 0.8 constant_dynamic-slice_fusion
  5.3 0.1 copy.42
  5.4 0.8 constant_dynamic-slice_fusion.2
  6.2 0.1 copy.46
  6.3 0.1 fusion.38
  6.4 0.0 copy-start.9
  6.4 0.1 copy.41
  6.5 0.1 multiply_cosine_fusion.1
  6.6 0.9 fusion.30
  7.5 0.1 concatenate.13.refs_0_
  7.6 1.0 %fusion.18.refs_1_ = bf16[32,2048]{1,0:T(8,128)(2,1)S(1)} fusion(f32[2048]{0:T(1024)} %param.29, f32[32]{0:T(128)S(1)} %add_rsqrt_fusion.1, bf16[128,2048]{1,0:T(8,128)(2,1)} %param.28, s32[]{:T(128)S(6)} %select_n.17), kind=kLoop, calls=%fused_computation.27 | loop fusion | flops 262144 | bytes 270468 | tf_op jit(solution)/shard_map/convert_element_type | solution.py:23
  8.6 1.6 %fusion.19 = f32[128,384]{0,1:T(8,128)S(1)} fusion(bf16[768,384]{1,0:T(8,128)(2,1)} %param.24, bf16[128,768]{1,0:T(8,128)(2,1)} %param.19, f32[768]{0:T(1024)} %param.22, f32[128]{0:T(128)S(1)} %add_rsqrt_fusion), kind=kOutput, calls=%fused_computation.28 | convolution fusion | flops 75890688 | bytes 986624 | tf_op jit(solution)/shard_map/dot_general | solution.py:700
  10.3 35.1 %shard_map.194 = (bf16[1024,640]{1,0:T(8,128)(2,1)S(1)}, bf16[1024,2048]{1,0:T(8,128)(2,1)S(1)}) custom-call(bf16[32,640]{1,0:T(8,128)(2,1)S(1)} %concatenate.13.refs_0_, bf16[32,2048]{1,0:T(8,128)(2,1)S(1)} %fusion.18.refs_1_), custom_call_target="tpu_custom_call" | custom-call | tf_op jit(solution)/shard_map/pallas_call | solution.py:382
  45.4 0.0 copy-start.1
  45.4 1.9 %copy-done.1 = bf16[1024,2048]{1,0:T(8,128)(2,1)} copy-done((bf16[1024,2048]{1,0:T(8,128)(2,1)}, bf16[1024,2048]{1,0:T(8,128)(2,1)S(1)}, u32[]{:S(2)}) %copy-start.1) | copy-done | bytes 4194328
  47.4 0.1 copy.44
  47.5 0.2 convert_add_fusion.scale_ref
  47.7 0.0 copy-done.9
  47.7 0.8 convolution_convert_fusion.1
  48.5 0.6 multiply_reduce_fusion
  49.1 0.0 copy-start.7
  49.1 0.5 fusion
  49.6 0.0 copy-start.2
  49.6 0.0 copy-start.3
  49.6 0.0 copy-start.4
  49.7 0.0 copy-start.5
  49.7 0.0 copy-start.6
  49.7 0.0 copy-start.8
  49.7 0.6 fusion.3
  50.3 0.0 copy-done
  50.3 0.3 convolution_convert_fusion.head_ref
  50.6 0.0 copy-done.7
  50.7 0.2 copy-done.2
  50.9 0.3 copy-done.3
  51.2 0.3 copy-done.4
  51.5 0.1 copy-done.5
  51.7 0.2 copy-done.6
  51.8 0.0 copy-done.8
  51.8 37.7 %shard_map.195 = (bf16[32,2048]{1,0:T(8,128)(2,1)S(1)}, bf16[128,512]{1,0:T(8,128)(2,1)S(1)}) custom-call(bf16[1024,2048]{1,0:T(8,128)(2,1)} %copy-done.1, f32[1024,1]{1,0:T(8,128)S(1)} %convert_add_fusion.scale_ref, bf16[2048,256]{1,0:T(8,128)(2,1)S(1)} %bitcast.18, bf16[2048,256]{1,0:T(8,128)(2,1)S(1)} %bitcast.19, bf16[256,2048]{1,0:T(8,128)(2,1)S(1)} %bitcast.20, ...), custom_call_target="tpu_custom_call" | custom-call | tf_op jit(solution)/shard_map/pallas_call | solution.py:611
  89.6 0.7 copy.49
  90.2 0.7 copy.50
  (16 shorter events, 0.2 us)
Async XLA Ops:
  0.6 49.7 %copy-start = (bf16[256,2048]{1,0:T(8,128)(2,1)S(1)}, bf16[256,2048]{1,0:T(8,128)(2,1)}, u32[]{:S(2)}) copy-start(bf16[256,2048]{1,0:T(8,128)(2,1)} %param.26) | copy-start | bytes 3145732
  6.4 41.3 %copy-start.9 = (bf16[512,512]{1,0:T(8,128)(2,1)S(1)}, bf16[512,512]{1,0:T(8,128)(2,1)}, u32[]{:S(2)}) copy-start(bf16[512,512]{1,0:T(8,128)(2,1)} %param.25) | copy-start | bytes 1572868
  45.4 1.9 %copy-start.1 = (bf16[1024,2048]{1,0:T(8,128)(2,1)}, bf16[1024,2048]{1,0:T(8,128)(2,1)S(1)}, u32[]{:S(2)}) copy-start(bf16[1024,2048]{1,0:T(8,128)(2,1)S(1)} %get-tuple-element.4.rows_ref) | copy-start | bytes 12582916
  49.1 1.5 %copy-start.7 = (bf16[128,2048]{1,0:T(8,128)(2,1)S(1)}, bf16[128,2048]{1,0:T(8,128)(2,1)}, u32[]{:S(2)}) copy-start(bf16[128,2048]{1,0:T(8,128)(2,1)} %shared_down_ref.1) | copy-start | bytes 1572868
  49.6 1.3 %copy-start.2 = (bf16[1,2048,256]{2,1,0:T(8,128)(2,1)S(1)}, bf16[1,2048,256]{2,1,0:T(8,128)(2,1)}, u32[]{:S(2)}) copy-start(bf16[1,2048,256]{2,1,0:T(8,128)(2,1)} %param.32) | copy-start | bytes 3145732
  49.6 1.6 %copy-start.3 = (bf16[1,2048,256]{2,1,0:T(8,128)(2,1)S(1)}, bf16[1,2048,256]{2,1,0:T(8,128)(2,1)}, u32[]{:S(2)}) copy-start(bf16[1,2048,256]{2,1,0:T(8,128)(2,1)} %param.33) | copy-start | bytes 3145732
  49.6 1.9 %copy-start.4 = (bf16[1,256,2048]{2,1,0:T(8,128)(2,1)S(1)}, bf16[1,256,2048]{2,1,0:T(8,128)(2,1)}, u32[]{:S(2)}) copy-start(bf16[1,256,2048]{2,1,0:T(8,128)(2,1)} %param.34) | copy-start | bytes 3145732
  49.7 2.0 %copy-start.5 = (bf16[2048,128]{1,0:T(8,128)(2,1)S(1)}, bf16[2048,128]{1,0:T(8,128)(2,1)}, u32[]{:S(2)}) copy-start(bf16[2048,128]{1,0:T(8,128)(2,1)} %shared_gate_ref.1) | copy-start | bytes 1572868
  49.7 2.1 %copy-start.6 = (bf16[2048,128]{1,0:T(8,128)(2,1)S(1)}, bf16[2048,128]{1,0:T(8,128)(2,1)}, u32[]{:S(2)}) copy-start(bf16[2048,128]{1,0:T(8,128)(2,1)} %shared_up_ref.1) | copy-start | bytes 1572868
  49.7 2.1 %copy-start.8 = (f32[2048]{0:T(1024)S(1)}, f32[2048]{0:T(1024)}, u32[]{:S(2)}) copy-start(f32[2048]{0:T(1024)} %param.27) | copy-start | bytes 24580
where the time goes:
time: 91.3 us; the launch traced here: 90.9 us
  Pallas kernels  72.9 us (80%)
  local copies, waits for them, and re-layouts  7.28 us (8%)
  other arithmetic  6.01 us (7%)
  matrix products  3.84 us (4%)
    pallas_call x1, Pallas kernels, reduce_all(): pl.pallas_call(functools.partial(reduce_kernel, dims), out_shape=[jax.Sha...  37.7 us
    pallas_call x1, Pallas kernels, gather_all(): pl.pallas_call(functools.partial(gather_kernel, dims), out_shape=[jax.Sha...  35.1 us
    unnamed x23, local copies, waits for them, and re-layouts  4.52 us
    reduce_sum x3, other arithmetic, rms_scale(): jnp.mean(widened * widened, -1, keepdims=True) + EPS  3.05 us
    convert_element_type x2, other arithmetic, rms_scale(): return (normed * gain_vec).astype(jnp.bfloat16)  1.88 us

commit v1 on v0

v1 whole, which is shorter than its diff:
```python
import functools
import math

import jax
import jax.numpy as jnp
import numpy as np
from jax import lax
from jax.experimental import pallas as pl
from jax.experimental.pallas import tpu as pltpu
from jax.sharding import PartitionSpec as P

NOPE = 64
ROPE = 32
VDIM = 64


EPS = 1e-06
ROPE_BASE = 10000.0


def rms_scale(values, gain_vec):
    widened = values.astype(jnp.float32)
    normed = widened * lax.rsqrt(jnp.mean(widened * widened, -1, keepdims=True) + EPS)
    return (normed * gain_vec).astype(jnp.bfloat16)


def rotate(values, positions):
    half_width = values.shape[-1] // 2
    inverse = 1.0 / ROPE_BASE ** (
        jnp.arange(half_width, dtype=jnp.float32) * 2.0 / (2 * half_width)
    )
    angles = positions[:, None] * inverse[None, :]
    cosine = jnp.cos(angles)
    sine_vals = jnp.sin(angles)
    if values.ndim == 3:
        cosine = cosine[:, None, :]
        sine_vals = sine_vals[:, None, :]
    first_half = values[..., :half_width]
    second = values[..., half_width:]
    return jnp.concatenate(
        [first_half * cosine - second * sine_vals, first_half * sine_vals + second * cosine], -1
    )


def per_device_slots(
    query_latent,
    keyval_latent,
    rotary_key,
    query_gain,
    keyval_gain,
    query_weight,
    keyval_weight,
    output_weight,
    output_gain,
    second_rows,
    second_gain,
    route_ids,
    route_weights,
    gate_weight,
    up_weight,
    down_weight,
    shared_gate,
    shared_up,
    shared_down,
):
    first_rows = query_latent.shape[0]
    tp_count = lax.axis_size("tp")
    ep_count = lax.axis_size("ep")
    head_count = query_weight.shape[1] // (NOPE + ROPE)
    positions = (lax.axis_index("ep") * first_rows).astype(jnp.float32) + jnp.arange(
        first_rows, dtype=jnp.float32
    )
    queries = jnp.dot(
        rms_scale(query_latent, query_gain), query_weight, preferred_element_type=jnp.float32
    ).reshape(first_rows, head_count, NOPE + ROPE)
    queries = jnp.concatenate(
        [queries[..., :NOPE], rotate(queries[..., NOPE:], positions)], -1
    ).astype(jnp.bfloat16)
    query_plain = queries[..., :NOPE]
    query_turned = queries[..., NOPE:]
    kv_normed = rms_scale(keyval_latent, keyval_gain)
    key_rot = rotate(rotary_key.astype(jnp.float32), positions).astype(jnp.bfloat16)
    score_scale = (NOPE + ROPE) ** (-0.5)

    def attend(carried, pieces):
        highest, denominator, accumulated = carried
        keyval_piece, rot_piece = pieces
        key_count = keyval_piece.shape[0]
        keyval_heads = keyval_piece.reshape(key_count, head_count, NOPE + VDIM)
        scores = jnp.einsum(
            "qhd,khd->hqk",
            query_plain,
            keyval_heads[..., :NOPE],
            preferred_element_type=jnp.float32,
        )
        scores = (
            scores
            + jnp.einsum("qhr,kr->hqk", query_turned, rot_piece, preferred_element_type=jnp.float32)
        ) * score_scale
        new_high = jnp.maximum(highest, jnp.max(scores, -1))
        exponent = jnp.exp(scores - new_high[..., None])
        rescale = jnp.exp(highest - new_high)
        denominator = denominator * rescale + jnp.sum(exponent, -1)
        update = jnp.einsum(
            "hqk,khe->qhe",
            exponent.astype(jnp.bfloat16),
            keyval_heads[..., NOPE:],
            preferred_element_type=jnp.float32,
        )
        accumulated = accumulated * rescale.T[..., None] + update
        return (new_high, denominator, accumulated)

    start_state = (
        jnp.full((head_count, first_rows), -jnp.inf, jnp.float32),
        jnp.zeros((head_count, first_rows), jnp.float32),
        jnp.zeros((first_rows, head_count, VDIM), jnp.float32),
    )
    quarter = first_rows // tp_count
    offset = lax.axis_index("tp") * quarter
    own_latent = lax.dynamic_slice_in_dim(kv_normed, offset, quarter, 0)
    own_rot = lax.dynamic_slice_in_dim(key_rot, offset, quarter, 0)
    all_latent, all_rot = (
        lax.all_gather(own_latent, ("ep", "tp"), axis=0, tiled=True),
        lax.all_gather(own_rot, ("ep", "tp"), axis=0, tiled=True),
    )
    total_keys = all_latent.shape[0]
    key_block = math.gcd(total_keys, 512)
    latent_blocks = all_latent.reshape(total_keys // key_block, key_block, all_latent.shape[1])
    rot_blocks = all_rot.reshape(total_keys // key_block, key_block, all_rot.shape[1])

    def scan_step(carried, block_pair):
        projected = jnp.dot(
            block_pair[0], keyval_weight, preferred_element_type=jnp.float32
        ).astype(jnp.bfloat16)
        return (attend(carried, (projected, block_pair[1])), None)

    final_state, _ = lax.scan(scan_step, start_state, (latent_blocks, rot_blocks))
    denominator = final_state[1]
    accumulated = final_state[2]
    attended = (
        (accumulated / denominator.T[..., None])
        .astype(jnp.bfloat16)
        .reshape(first_rows, head_count * VDIM)
    )
    mixture = lax.psum_scatter(
        jnp.dot(attended, output_weight, preferred_element_type=jnp.float32).astype(jnp.bfloat16),
        "tp",
        scatter_dimension=0,
        tiled=True,
    ).astype(jnp.float32)
    mixed = rms_scale(mixture, output_gain)
    tok_rows = second_rows.shape[0]
    model_width = second_rows.shape[1]
    top_count = route_ids.shape[1]
    local_count = gate_weight.shape[0]
    expert_count = local_count * ep_count
    capacity = max(tp_count, tok_rows * top_count * 2 // expert_count // tp_count * tp_count)
    normed = rms_scale(second_rows, second_gain)
    flat_ids = route_ids.reshape(-1)
    onehot = (flat_ids[:, None] == jnp.arange(expert_count, dtype=jnp.int32)[None, :]).astype(
        jnp.int32
    )
    slot_rank = jnp.sum((jnp.cumsum(onehot, 0) - 1) * onehot, 1)
    owners = jnp.arange(tok_rows * top_count, dtype=jnp.int32) // top_count
    slot_table = (
        jnp.full((expert_count * capacity,), tok_rows, jnp.int32)
        .at[flat_ids * capacity + slot_rank]
        .set(owners)
    )
    padded = jnp.concatenate([normed, jnp.zeros((1, model_width), jnp.bfloat16)], 0)
    outgoing = padded[slot_table].reshape(ep_count, local_count, capacity, model_width)
    weights = route_weights.reshape(-1, 1)
    shared_hidden = (
        jax.nn.silu(jnp.dot(normed, shared_gate, preferred_element_type=jnp.float32))
        * jnp.dot(normed, shared_up, preferred_element_type=jnp.float32)
    ).astype(jnp.bfloat16)
    shared_part = jnp.dot(shared_hidden, shared_down, preferred_element_type=jnp.float32)
    arrived = lax.all_to_all(outgoing, "ep", split_axis=0, concat_axis=0, tiled=True)
    gate_act = jnp.einsum(
        "sicd,idf->sicf", arrived, gate_weight, preferred_element_type=jnp.float32
    )
    up_act = jnp.einsum("sicd,idf->sicf", arrived, up_weight, preferred_element_type=jnp.float32)
    hidden = (jax.nn.silu(gate_act) * up_act).astype(jnp.bfloat16)
    slot_terms = jnp.einsum(
        "sicf,ifd->sicd", hidden, down_weight, preferred_element_type=jnp.float32
    ).reshape(-1, model_width)
    slot_sum, shared_sum = (
        lax.psum_scatter(
            slot_terms.astype(jnp.bfloat16), "tp", scatter_dimension=1, tiled=True
        ).astype(jnp.float32),
        lax.psum_scatter(
            shared_part.astype(jnp.bfloat16), "tp", scatter_dimension=1, tiled=True
        ).astype(jnp.float32),
    )
    column_part = model_width // tp_count
    returned = lax.all_to_all(
        slot_sum.astype(jnp.bfloat16).reshape(ep_count, local_count * capacity, column_part),
        "ep",
        split_axis=0,
        concat_axis=0,
        tiled=True,
    )
    returned = returned.reshape(expert_count * capacity, column_part)
    picked = returned[flat_ids * capacity + slot_rank].astype(jnp.float32) * weights
    routed = jnp.sum(picked.reshape(tok_rows, top_count, column_part), 1)
    expert_mix = (routed + shared_sum).astype(jnp.bfloat16)
    return (mixed, expert_mix)


MESH = pl.DeviceIdType.MESH
LANES = 128


def grid_of(ep_count, tp_count):
    y_count = math.gcd(ep_count, 2)
    k_count = math.gcd(tp_count, 2)
    return (ep_count // y_count, y_count, tp_count // k_count, k_count)


def place_of(dims):
    ep_at, tp_at = lax.axis_index("ep"), lax.axis_index("tp")
    return (
        lax.div(ep_at, dims[1]),
        lax.rem(ep_at, dims[1]),
        lax.div(tp_at, dims[3]),
        lax.rem(tp_at, dims[3]),
    )


def moved(dims, place, dz=0, dy=0, dx=0, dk=0):
    return tuple(
        lax.rem(at + step % size, size) if step % size else at
        for at, step, size in zip(place, (dz, dy, dx, dk), dims)
    )


def device_of(dims, place):
    return (place[0] * dims[1] + place[1], place[2] * dims[3] + place[3])


def block_of(dims, place):
    ep_at, tp_at = device_of(dims, place)
    return ep_at * (dims[2] * dims[3]) + tp_at


def line_order(z_at, count):
    least = jnp.minimum(z_at, count - 1 - z_at)
    order = [z_at]
    for turn in range(1, count):
        far = turn > 2 * least
        step = jnp.where(far, turn - least, (turn + 1) // 2)
        down = jnp.where(far, 2 * z_at >= count, turn % 2 == 1)
        order.append(jnp.where(down, z_at - step, z_at + step))
    return order


LAT, TOK = 0, 1
A, B, C, D = "A", "B", "C", "D"
KA, KB, KC, KD = "kA", "kB", "kC", "kD"
QUERY, PROJECT, ATTEND, HEAD_OUT, MIX_SEND, MIX_DONE = range(10, 16)
EXPERTS, FAR, SIDE_X, SIDE_Y, OWN = range(16, 21)
SCHEDULE = (
    (LAT, C, 0, 0), (TOK, A, 1, 0), (LAT, A, 1, 0), (TOK, A, 2, 0), (TOK, C, 0, 1),
    (TOK, B, 1, 0), (TOK, A, 1, 1), (LAT, A, 2, 0), (TOK, B, 2, 0), (TOK, A, 2, 1),
    (TOK, C, 0, 0), (TOK, B, 1, 1), (TOK, C, 2, 0), (TOK, KC, 0, 0), (EXPERTS, 0, 0),
    (LAT, B, 1, 0), (LAT, C, 2, 0), (TOK, C, 1, 1), (TOK, D, 0, 0), (TOK, D, 0, 1),
    (TOK, C, 2, 1), (TOK, A, 3, 0), (TOK, D, 2, 0), (TOK, D, 1, 1), (LAT, A, 3, 0),
    (LAT, B, 2, 0), (LAT, D, 0, 0), (LAT, KC, 2, 0), (TOK, A, 3, 1), (LAT, C, 1, 0),
    (TOK, KD, 2, 0), (LAT, D, 1, 0), (LAT, D, 2, 0), (LAT, KC, 1, 0), (TOK, B, 2, 1),
    (TOK, D, 2, 1), (TOK, KC, 0, 1), (TOK, KB, 2, 0), (LAT, KD, 2, 0), (TOK, KA, 2, 1), (QUERY,),
    (TOK, KB, 2, 1), (TOK, C, 1, 0), (TOK, KA, 2, 0), (TOK, C, 3, 0), (LAT, KD, 0, 0),
    (LAT, KA, 2, 0), (LAT, KB, 2, 0), (TOK, KC, 2, 0), (TOK, KA, 1, 0), (LAT, KB, 1, 0),
    (TOK, KD, 0, 1), (TOK, KC, 1, 1), (LAT, KD, 1, 0), (TOK, B, 3, 0), (TOK, D, 1, 0),
    (TOK, KA, 3, 1), (TOK, KC, 2, 1), (TOK, KD, 1, 1), (TOK, KD, 2, 1), (LAT, C, 3, 0),
    (EXPERTS, 2, 1), (TOK, C, 3, 1), (EXPERTS, 2, 0), (LAT, KC, 3, 0), (TOK, KC, 1, 0),
    (LAT, B, 3, 0), (FAR, 2), (TOK, KD, 1, 0), (TOK, B, 3, 1), (TOK, KD, 0, 0), (EXPERTS, 1, 1),
    (LAT, KC, 0, 0), (TOK, KC, 3, 1), (FAR, 1), (LAT, D, 3, 0), (TOK, KA, 3, 0), (LAT, KB, 3, 0),
    (TOK, KA, 1, 1), (TOK, D, 3, 1), (TOK, D, 3, 0), (EXPERTS, 0, 1), (TOK, KC, 3, 0),
    (LAT, KA, 3, 0), (SIDE_X, 2), (TOK, KB, 1, 1), (SIDE_Y, 2), (TOK, KD, 3, 0), (TOK, KB, 1, 0),
    (LAT, KA, 1, 0), (EXPERTS, 1, 0), (LAT, KD, 3, 0), (TOK, KD, 3, 1), (TOK, KB, 3, 0),
    (EXPERTS, 3, 1), (FAR, 0), (TOK, KB, 3, 1), (PROJECT,), (ATTEND, 3), (FAR, 3), (SIDE_X, 1),
    (SIDE_Y, 1), (OWN, 2), (EXPERTS, 3, 0), (SIDE_X, 3), (SIDE_Y, 3), (SIDE_Y, 0), (SIDE_X, 0),
    (ATTEND, 0), (ATTEND, 2), (OWN, 1), (ATTEND, 1), (HEAD_OUT,), (OWN, 3), (MIX_SEND,), (OWN, 0),
    (MIX_DONE,),
)
OVER_Y = ((0, 1, 0), (1, 0, 0), (1, 1, 0), (1, 1, 1), (1, 3, 0),)
CHUNKS = (1, 2)
B_OVER_Z = (False, True)
C_OVER_Z = (False, True)
LAST_TURN = max(entry[2] for entry in SCHEDULE if entry[0] in (LAT, TOK))


def relay_way(which, turn, chunk):
    return "y" if (which, turn, chunk) in OVER_Y else "x"


def gather_keys(dims):
    keys = []
    for which in range(2):
        for turn in range(dims[0]):
            names = ["C", "D", "kC", "kD"]
            names += ["F", "B", "kA", "kB"] if turn else ["L", "R", "BL", "BR", "CL", "CR"]
            keys += [(which, n, turn, c) for n in names for c in range(CHUNKS[which])]
    return {key: index for index, key in enumerate(keys)}


def reduce_keys(dims):
    keys = []
    for turn in range(dims[0]):
        keys += [("k", turn, dy, dx) for dy in range(2) for dx in range(2)]
        keys += [("p", turn), ("q", turn), ("x", turn), ("y", turn)]
    keys += [("mk", 0), ("mk", 1), ("mx", 0)]
    return {key: index for index, key in enumerate(keys)}


def reduce_slots(dims):
    slots, sizes = {}, {"half": 0, "mix": 0, "full": 0}
    for key in reduce_keys(dims):
        group = "half" if key[0] in "pq" else ("mix" if key[0][0] == "m" else "full")
        slots[key] = (group, sizes[group])
        sizes[group] += 1
    return slots, sizes


LOADS = (
    "kl",
    "kg",
    "rk",
    "tab",
    "rid",
    "rwt",
    "sr",
    "sg",
    "ql",
    "qg",
    "qw",
    "gate",
    "up",
    "shg",
    "shu",
    "down",
    "shd",
    "kw",
    "ow",
    "og",
)


def layer_kernel(dims, names, *refs):
    ref = dict(zip(names, refs))
    z_count = dims[0]
    me = place_of(dims)
    ep_at = lax.axis_index("ep")
    ep_count = dims[0] * dims[1]
    g_keys, r_keys = gather_keys(dims), reduce_keys(dims)
    slots, _ = reduce_slots(dims)
    zs = line_order(me[0], z_count)
    lat, tok = ref["lat_all"], ref["tok_all"]
    alls = (lat, tok)
    rows = ref["v_sr"].shape[0]
    quarter = rows // (dims[2] * dims[3])
    latent_width = ref["v_kl"].shape[1]
    tile_at = pl.ds(latent_width, LANES)
    head_count = ref["v_qw"].shape[1] // (NOPE + ROPE)
    own_rows = pl.ds(pl.multiple_of(ep_at * rows, rows), rows)
    sent = []

    local = {}
    for number, name in enumerate(LOADS):
        source, target = ref["h_" + name], ref["v_" + name] if "v_" + name in ref else None
        if name == "tab":
            source = source.at[:, own_rows]
        elif name in ("gate", "up", "down"):
            source = source.at[0]
        if name in ("gate", "up"):
            width = source.shape[1]
            target = ref["v_gu"].at[:, pl.ds(width * (name == "up"), width)]
        elif name in ("shg", "shu"):
            width = source.shape[1]
            target = ref["v_sgu"].at[:, pl.ds(width * (name == "shu"), width)]
        local[name] = pltpu.make_async_copy(source, target, ref["load_sem"].at[number])
        local[name].start()

    def loaded(*wanted):
        for name in wanted:
            local[name].wait()

    barrier = pltpu.get_barrier_semaphore()
    peers = [{"dz": dz} for dz in range(1, z_count)] + [{"dy": 1}, {"dx": 1}, {"dk": 1}]
    for peer in peers:
        pl.semaphore_signal(
            barrier,
            inc=1,
            device_id=device_of(dims, moved(dims, me, **peer)),
            device_id_type=MESH,
        )

    def at_place(turn, dy=0, dx=0, dk=0):
        return (zs[turn],) + moved(dims, me, dy=dy, dx=dx, dk=dk)[1:]

    def region(which, place, chunk):
        size = quarter // CHUNKS[which]
        begin = pl.multiple_of(block_of(dims, place) * quarter + chunk * size, size)
        return alls[which].at[pl.ds(begin, size), :]

    def place_from(name, turn):
        return at_place(turn, *{"A": (0, 0), "B": (0, 1), "C": (1, 0), "D": (1, 1)}[name[-1]])[
            :3
        ] + ((moved(dims, me, dk=1) if name[0] == "k" else me)[3],)

    def g_copy(key, place, target):
        at = region(key[0], place, key[3])
        return pltpu.make_async_remote_copy(
            src_ref=at,
            dst_ref=at,
            send_sem=ref["g_send"].at[g_keys[key]],
            recv_sem=ref["g_recv"].at[g_keys[key]],
            device_id=device_of(dims, target),
            device_id_type=MESH,
        )

    def g_send(key, place, **step):
        copy = g_copy(key, place, moved(dims, me, **step))
        copy.start()
        sent.append(copy)

    def line_copy(which, key, place, chunk, target_z):
        at = region(which, place, chunk)
        kind = "BC".find(key[1][0]) + 1
        return pltpu.make_async_remote_copy(
            src_ref=at,
            dst_ref=at,
            send_sem=ref["g_send"].at[g_keys[key]],
            recv_sem=ref["line_recv"].at[which * 3 + kind, place[0], chunk],
            device_id=device_of(dims, (target_z,) + me[1:]),
            device_id_type=MESH,
        )

    line_sent = []

    def line_send(key, place, down):
        target = jnp.where(down, me[0] - 1, me[0] + 1)
        there = (target >= 0) & (target < z_count)
        if key[1][0] in "BC":
            there &= line_order(target, z_count)[1] == me[0]
        copy = line_copy(key[0], key, place, key[3], jnp.where(there, target, me[0]))

        @pl.when(there)
        def _():
            copy.start()

        line_sent.append((there, copy))

    def take(which, name, turn, chunk):
        place = place_from(name, turn)
        if name == "A":
            key = (which, "F", turn, chunk)
            line_copy(which, key, place, chunk, me[0]).wait_recv()
            line_send(key, place, place[0] > me[0])
            if not (turn == 1 and B_OVER_Z[which]):
                g_send((which, "B", turn, chunk), place, dx=1)
            if not (turn == 1 and C_OVER_Z[which]):
                g_send((which, "C", turn, chunk), place, dy=1)
        elif turn == 1 and (name == "B" and B_OVER_Z[which] or name == "C" and C_OVER_Z[which]):
            line_copy(which, (which, name + "L", 0, chunk), place, chunk, me[0]).wait_recv()
        else:
            g_copy((which, name, turn, chunk), place, me).wait_recv()
        if name == "C" and turn == 0 and C_OVER_Z[which]:
            line_send((which, "CL", 0, chunk), place, True)
            line_send((which, "CR", 0, chunk), place, False)
        way = relay_way(which, turn, chunk)
        if name == "B" and turn and way == "y":
            g_send((which, "D", turn, chunk), place, dy=1)
        if name == "C" and way == "x":
            g_send((which, "D", turn, chunk), place, dx=1)
        if name[0] != "k":
            g_send((which, "k" + name, turn, chunk), place, dk=1)

    def rms(values, gain):
        widened = values.astype(jnp.float32)
        scale = lax.rsqrt(jnp.mean(widened * widened, -1, keepdims=True) + EPS)
        return (widened * scale * gain).astype(jnp.bfloat16)

    lane = lax.broadcasted_iota(jnp.int32, (rows, LANES), 1)

    loaded("kl", "kg", "rk", "tab", "rid", "rwt")
    lat[own_rows, pl.ds(0, latent_width)] = rms(ref["v_kl"][...], ref["v_kg"][...].reshape(1, -1))
    half = ROPE // 2
    turned = ref["v_rk"][...].astype(jnp.float32)
    cos_t, sin_t = ref["v_tab"][pl.ds(0, half), :], ref["v_tab"][pl.ds(half, half), :]
    first, second = turned[:half], turned[half:]
    expert = lax.broadcasted_iota(jnp.int32, (ep_count, rows), 0)
    dense = jnp.zeros((ep_count, rows), jnp.float32)
    for choice in range(ref["v_rid"].shape[0]):
        picked = ref["v_rid"][pl.ds(choice, 1), :] == expert
        dense += jnp.where(picked, ref["v_rwt"][pl.ds(choice, 1), :], 0.0)
    high = dense.astype(jnp.bfloat16).astype(jnp.float32)
    upright = jnp.concatenate(
        [
            high,
            dense - high,
            jnp.zeros((NOPE - 2 * ep_count, rows), jnp.float32),
            first * cos_t - second * sin_t,
            first * sin_t + second * cos_t,
            jnp.zeros((LANES - NOPE - ROPE, rows), jnp.float32),
        ],
        0,
    )
    lat[own_rows, tile_at] = upright.T.astype(jnp.bfloat16)

    pl.semaphore_wait(barrier, len(peers))

    def send_own(which):
        for chunk in range(CHUNKS[which]):
            line_send((which, "L", 0, chunk), me, True)
            line_send((which, "R", 0, chunk), me, False)
            g_send((which, "C", 0, chunk), me, dy=1)

    def send_mirror(which):
        for chunk in range(CHUNKS[which]):
            if relay_way(which, 0, chunk) == "y":
                g_send((which, "D", 0, chunk), at_place(0, 0, 1), dy=1)
            if B_OVER_Z[which]:
                line_send((which, "BL", 0, chunk), at_place(0, 0, 1), True)
                line_send((which, "BR", 0, chunk), at_place(0, 0, 1), False)

    send_own(0)
    send_mirror(0)
    loaded("sr", "sg")

    def norm_quarter(place):
        begin = pl.multiple_of(device_of(dims, place)[1] * quarter, quarter)
        target = pl.multiple_of(block_of(dims, place) * quarter, quarter)
        tok[pl.ds(target, quarter), :] = rms(
            ref["v_sr"][pl.ds(begin, quarter), :], ref["v_sg"][...].reshape(1, -1)
        )

    norm_quarter(me)
    send_own(1)
    norm_quarter(moved(dims, me, dx=1))
    send_mirror(1)
    for dx, dk in ((0, 1), (1, 1)):
        norm_quarter(moved(dims, me, dx=dx, dk=dk))

    def make_queries():
        loaded("ql", "qg", "qw")
        product = jnp.dot(
            rms(ref["v_ql"][...], ref["v_qg"][...].reshape(1, -1)),
            ref["v_qw"][...],
            preferred_element_type=jnp.float32,
        )
        blank = jnp.zeros((NOPE, rows), jnp.float32)
        tail = jnp.zeros((LANES - NOPE - ROPE, rows), jnp.float32)
        cos_tile = jnp.concatenate([blank, cos_t, cos_t, tail], 0).T
        sin_tile = jnp.concatenate([blank, -sin_t, sin_t, tail], 0).T
        wide = product.shape[1]
        for head in range(head_count):
            begin = head * (NOPE + ROPE)
            part = pltpu.roll(product, (wide - begin) % wide, 1)[:, :LANES]
            swapped = jnp.where(
                lane < NOPE + half, pltpu.roll(part, LANES - half, 1), pltpu.roll(part, half, 1)
            )
            ref["q_all"][head, :, pl.ds(0, LANES)] = jnp.where(lane < NOPE, part, 0.0).astype(
                jnp.bfloat16
            )
            ref["q_all"][head, :, pl.ds(LANES, LANES)] = (
                part * cos_tile + swapped * sin_tile
            ).astype(jnp.bfloat16)

    outs = [None] * head_count

    def project():
        loaded("kw")
        ref["kv_all"][...] = jnp.dot(
            lat[:, pl.ds(0, latent_width)], ref["v_kw"][...], preferred_element_type=jnp.float32
        ).astype(jnp.bfloat16)

    def attend(head):
        own = ref["kv_all"][:, pl.ds(head * LANES, LANES)]
        keys = jnp.concatenate([own, lat[:, tile_at]], 1)
        scores = lax.dot_general(
            ref["q_all"][head],
            keys,
            (((1,), (1,)), ((), ())),
            preferred_element_type=jnp.float32,
        ) * ((NOPE + ROPE) ** (-0.5))
        exponent = jnp.exp(scores - jnp.max(scores, -1, keepdims=True))
        denominator = jnp.sum(exponent, -1, keepdims=True)
        outs[head] = (
            jnp.dot(exponent.astype(jnp.bfloat16), own, preferred_element_type=jnp.float32)
            / denominator
        )

    def mix_span(dx, dk):
        size = ref["mixed"].shape[0]
        begin = device_of(dims, moved(dims, me, dx=dx, dk=dk))[1] * size
        return pl.ds(pl.multiple_of(begin, size), size)

    stores = {"half": ref["halves"], "mix": ref["mixes"], "full": ref["full"]}

    def r_copy(key, source, target):
        group, index = slots[key]
        return pltpu.make_async_remote_copy(
            src_ref=source,
            dst_ref=stores[group].at[index],
            send_sem=ref["r_send"].at[r_keys[key]],
            recv_sem=ref["r_recv"].at[r_keys[key]],
            device_id=device_of(dims, target),
            device_id_type=MESH,
        )

    def r_send(key, source, **step):
        copy = r_copy(key, source, moved(dims, me, **step))
        copy.start()
        sent.append(copy)

    def landed(key):
        group, index = slots[key]
        at = stores[group].at[index]
        r_copy(key, at, me).wait_recv()
        return at[...].astype(jnp.float32)

    def head_out():
        loaded("ow")
        pairs = [
            jnp.where(lane < VDIM, pltpu.roll(outs[head], VDIM, 1), outs[head + 1])
            for head in range(0, head_count, 2)
        ]
        attended = jnp.concatenate(pairs, 1).astype(jnp.bfloat16)
        ref["head"][...] = jnp.dot(
            attended, ref["v_ow"][...], preferred_element_type=jnp.float32
        ).astype(jnp.bfloat16)
        for dx in (1, 0):
            r_send(("mk", dx), ref["head"].at[mix_span(dx, 1)], dk=1)

    def mix_core(dx):
        return ref["head"][mix_span(dx, 0), :].astype(jnp.float32) + landed(("mk", dx))

    def mix_send():
        ref["mix_sum"][...] = mix_core(1).astype(jnp.bfloat16)
        r_send(("mx", 0), ref["mix_sum"], dx=1)

    def mix_done():
        loaded("og")
        mixture = mix_core(0) + landed(("mx", 0))
        scale = lax.rsqrt(jnp.mean(mixture * mixture, -1, keepdims=True) + EPS)
        ref["mixed"][...] = (mixture * scale * ref["v_og"][...].reshape(1, -1)).astype(jnp.bfloat16)

    parts, sums = ref["parts"], ref["sums"]
    part_width = ref["out"].shape[1]

    def part_of(dz, dy, dx, dk):
        column = device_of(dims, moved(dims, me, dx=dx, dk=dk))[1]
        return parts.at[dz * 2 + dy, column]

    def gated(both):
        width = both.shape[1] // 2
        gate_act, up_act = both[:, :width], both[:, width:]
        return gate_act / (1.0 + jnp.exp(-gate_act)) * up_act

    def experts(dz, dy):
        begin = device_of(dims, at_place(dz, dy))[0] * rows
        span = pl.ds(pl.multiple_of(begin, rows), rows)
        tokens = tok[span, :]
        chosen = (lane == ep_at) | (lane == ep_count + ep_at)
        scale = jnp.sum(
            jnp.where(chosen, lat[span, tile_at].astype(jnp.float32), 0.0), -1, keepdims=True
        )
        if dz == 0 and dy == 0:
            loaded("gate", "up")
        both = jnp.dot(tokens, ref["v_gu"][...], preferred_element_type=jnp.float32)
        hidden = (gated(both) * scale).astype(jnp.bfloat16)
        own = dz == 0 and dy == 0
        if own:
            loaded("shg", "shu", "down", "shd")
            both = jnp.dot(tokens, ref["v_sgu"][...], preferred_element_type=jnp.float32)
            hidden_own = gated(both).astype(jnp.bfloat16)
        for column in range(dims[2] * dims[3]):
            columns = pl.ds(column * part_width, part_width)
            value = jnp.dot(
                hidden, ref["v_down"][:, columns], preferred_element_type=jnp.float32
            )
            if own:
                value += jnp.dot(
                    hidden_own, ref["v_shd"][:, columns], preferred_element_type=jnp.float32
                )
            parts[dz * 2 + dy, column] = value.astype(jnp.bfloat16)
        for dx in (1, 0):
            r_send(("k", dz, dy, dx), part_of(dz, dy, dx, 1), dk=1)

    def core_sum(dz, dy, dx):
        return part_of(dz, dy, dx, 0)[...].astype(jnp.float32) + landed(("k", dz, dy, dx))

    def keep(dz, dy, dx, value):
        index = dz * 4 + dy * 2 + dx
        sums[index] = value.astype(jnp.bfloat16)
        return sums.at[index]

    half_rows = rows // 2

    def finish_far(dz):
        at = keep(dz, 1, 1, core_sum(dz, 1, 1))
        r_send(("p", dz), at.at[pl.ds(0, half_rows)], dy=1)
        r_send(("q", dz), at.at[pl.ds(half_rows, half_rows)], dx=1)

    def finish_side_y(dz):
        value = core_sum(dz, 1, 0)
        value = jnp.concatenate([value[:half_rows], value[half_rows:] + landed(("q", dz))], 0)
        r_send(("y", dz), keep(dz, 1, 0, value), dy=1)

    def finish_side_x(dz):
        value = core_sum(dz, 0, 1)
        value = jnp.concatenate([value[:half_rows] + landed(("p", dz)), value[half_rows:]], 0)
        r_send(("x", dz), keep(dz, 0, 1, value), dx=1)

    final = []

    def z_copy(slot, source, target_z):
        return pltpu.make_async_remote_copy(
            src_ref=source,
            dst_ref=ref["line_parts"].at[slot],
            send_sem=ref["line_send"].at[slot],
            recv_sem=ref["line_done"].at[slot],
            device_id=device_of(dims, (target_z,) + me[1:]),
            device_id_type=MESH,
        )

    def finish_own(dz):
        value = core_sum(dz, 0, 0) + landed(("x", dz)) + landed(("y", dz))
        if dz:
            target = zs[dz]
            slot = lax.rem(me[0] - target + z_count, z_count)
            copy = z_copy(slot, keep(dz, 0, 0, value), target)
            copy.start()
            sent.append(copy)
        else:
            final.append(value)

    def z_landed(turn):
        slot = lax.rem(zs[turn] - me[0] + z_count, z_count)
        at = ref["line_parts"].at[slot]
        z_copy(slot, at, me[0]).wait_recv()
        return at[...].astype(jnp.float32)

    actions = {
        QUERY: make_queries,
        PROJECT: project,
        ATTEND: attend,
        HEAD_OUT: head_out,
        MIX_SEND: mix_send,
        MIX_DONE: mix_done,
        EXPERTS: experts,
        FAR: finish_far,
        SIDE_X: finish_side_x,
        SIDE_Y: finish_side_y,
        OWN: finish_own,
    }
    for entry in SCHEDULE:
        if entry[0] in actions:
            actions[entry[0]](*entry[1:])
        else:
            take(*entry)
    total = final[0]
    for turn in range(1, z_count):
        total = total + z_landed(turn)
    ref["out"][...] = total.astype(jnp.bfloat16)
    for there, copy in line_sent:
        pl.when(there)(copy.wait_send)
    for copy in sent:
        copy.wait_send()


def per_device_fused(ep_count, tp_count, *args):
    (ql, kl, rk, qg, kg, qw, kw, ow, og, sr, sg, rid, rwt, gate, up, down, shg, shu, shd) = args
    dims = grid_of(ep_count, tp_count)
    half = ROPE // 2
    rows, model_width = sr.shape
    angles = (
        np.arange(rows * ep_count, dtype=np.float64)[None, :]
        * ROPE_BASE ** (-np.arange(half, dtype=np.float64) / half)[:, None]
    )
    table = np.concatenate([np.cos(angles), np.sin(angles)], 0).astype(np.float32)
    given = {
        "kl": kl,
        "kg": kg,
        "rk": rk.T,
        "tab": jnp.asarray(table),
        "rid": rid.T,
        "rwt": rwt.T,
        "sr": sr,
        "sg": sg,
        "ql": ql,
        "qg": qg,
        "qw": qw,
        "gate": gate,
        "up": up,
        "shg": shg,
        "shu": shu,
        "down": down,
        "shd": shd,
        "kw": kw,
        "ow": ow,
        "og": og,
    }
    bf16 = jnp.bfloat16
    scratch = {
        "v_" + name: pltpu.VMEM(given[name].shape, given[name].dtype)
        for name in LOADS
        if name not in ("tab", "gate", "up", "down", "shg", "shu")
    }
    hidden = gate.shape[2]
    total = rows * ep_count
    width = model_width // tp_count
    mix_rows = rows // tp_count
    head_count = qw.shape[1] // (NOPE + ROPE)
    _, sizes = reduce_slots(dims)
    scratch |= {
        "v_tab": pltpu.VMEM((ROPE, rows), jnp.float32),
        "v_gu": pltpu.VMEM((model_width, 2 * hidden), bf16),
        "v_sgu": pltpu.VMEM((model_width, 2 * shg.shape[1]), bf16),
        "v_down": pltpu.VMEM(down.shape[1:], bf16),
        "lat_all": pltpu.VMEM((total, kl.shape[1] + LANES), bf16),
        "tok_all": pltpu.VMEM((total, model_width), bf16),
        "kv_all": pltpu.VMEM((total, kw.shape[1]), bf16),
        "q_all": pltpu.VMEM((head_count, rows, 2 * LANES), bf16),
        "head": pltpu.VMEM((rows, model_width), bf16),
        "parts": pltpu.VMEM((ep_count, tp_count, rows, width), bf16),
        "full": pltpu.VMEM((sizes["full"], rows, width), bf16),
        "halves": pltpu.VMEM((sizes["half"], rows // 2, width), bf16),
        "mixes": pltpu.VMEM((sizes["mix"], mix_rows, model_width), bf16),
        "sums": pltpu.VMEM((dims[0] * 4, rows, width), bf16),
        "mix_sum": pltpu.VMEM((mix_rows, model_width), bf16),
        "line_parts": pltpu.VMEM((dims[0], rows, width), bf16),
        "line_send": pltpu.SemaphoreType.DMA((dims[0],)),
        "line_done": pltpu.SemaphoreType.DMA((dims[0],)),
        "line_recv": pltpu.SemaphoreType.DMA((6, dims[0], max(CHUNKS))),
        "load_sem": pltpu.SemaphoreType.DMA((len(LOADS),)),
        "g_send": pltpu.SemaphoreType.DMA((len(gather_keys(dims)),)),
        "g_recv": pltpu.SemaphoreType.DMA((len(gather_keys(dims)),)),
        "r_send": pltpu.SemaphoreType.DMA((len(reduce_keys(dims)),)),
        "r_recv": pltpu.SemaphoreType.DMA((len(reduce_keys(dims)),)),
    }
    names = ["h_" + name for name in LOADS] + ["mixed", "out"] + list(scratch)
    vmem = pl.BlockSpec(memory_space=pltpu.VMEM)
    return pl.pallas_call(
        functools.partial(layer_kernel, dims, names),
        out_shape=[
            pltpu.VMEM((mix_rows, model_width), bf16),
            pltpu.VMEM((rows, width), bf16),
        ],
        in_specs=[pl.BlockSpec(memory_space=pltpu.HBM)] * len(LOADS),
        out_specs=[vmem] * 2,
        scratch_shapes=list(scratch.values()),
        compiler_params=pltpu.CompilerParams(
            collective_id=0, has_side_effects=True, vmem_limit_bytes=56 * 1024 * 1024
        ),
    )(*[given[name] for name in LOADS])


def solution(mesh):
    placed = (
        P("ep", None),
        P("ep", None),
        P("ep", None),
        P(),
        P(),
        P(None, "tp"),
        P(None, "tp"),
        P("tp", None),
        P(),
        P("ep", None),
        P(),
        P("ep", None),
        P("ep", None),
        P("ep", None, "tp"),
        P("ep", None, "tp"),
        P("ep", "tp", None),
        P(None, "tp"),
        P(None, "tp"),
        P("tp", None),
    )

    def per_device(*args):
        ep_count, tp_count = mesh.shape["ep"], mesh.shape["tp"]
        dims = grid_of(ep_count, tp_count)
        tok_rows, top_count = args[11].shape
        expert_count = args[13].shape[0] * ep_count
        capacity = tok_rows * top_count * 2 // expert_count
        head_count = args[5].shape[1] // (NOPE + ROPE)
        if (
            args[13].shape[0] == 1
            and capacity >= tok_rows
            and dims[0] == 1 + LAST_TURN
            and dims[1:] == (2, 2, 2)
            and tok_rows == args[0].shape[0] == LANES
            and head_count % 2 == 0
            and 2 * ep_count <= NOPE
        ):
            return per_device_fused(ep_count, tp_count, *args)
        return per_device_slots(*args)

    return jax.shard_map(
        per_device,
        mesh=mesh,
        in_specs=placed,
        out_specs=(P(("ep", "tp"), None), P("ep", "tp")),
        check_vma=False,
    )
```

time: 91.3 us -> 57.6 us (0.63)
  Pallas kernels: 72.9 us -> 55.5 us
  other arithmetic: 6.01 us -> 0 us
  local copies, waits for them, and re-layouts: 7.28 us -> 1.31 us
  matrix products: 3.84 us -> 0 us
    pallas_call x2 -> x1, Pallas kernels: 72.9 us -> 55.5 us  [per_device_fused(): pl.pallas_call(functools.partial(layer_kernel, dims, names), out_shape=[p...]
    dot_general x5 -> x0, matrix products: 3.84 us -> none  [the longest x1 1.6 us: per_device_dense(): jnp.dot(rms_scale(query_latent, query_gain), query_weight, preferred_elem...]
    reduce_sum x5 -> x0, other arithmetic: 3.57 us -> none  [the longest x3 3.05 us: rms_scale(): jnp.mean(widened * widened, -1, keepdims=True) + EPS]
    unnamed x23 -> x2, local copies, waits for them, and re-layouts: 4.52 us -> 1.31 us
    dynamic_slice x3 -> x0, local copies, waits for them, and re-layouts: 2.29 us -> none  [the longest x1 0.77 us: per_device_dense(): lax.dynamic_slice_in_dim(rotary_key, offset, quarter, 0).astype(jnp.float32)]
    convert_element_type x5 -> x0, other arithmetic: 1.9 us -> none  [the longest x2 1.88 us: rms_scale(): return (normed * gain_vec).astype(jnp.bfloat16)]
where the time goes in v1:
time: 57.6 us; the launch traced here: 57.5 us
  Pallas kernels  55.5 us (96%)
  local copies, waits for them, and re-layouts  1.31 us (2%)
  between operations  0.65 us (1%)
    pallas_call x1, Pallas kernels, per_device_fused(): pl.pallas_call(functools.partial(layer_kernel, dims, names), out_shape=[p...  55.5 us
    unnamed x2, local copies, waits for them, and re-layouts  1.31 us

profile of v1, /device:TPU:0, one launch (start us, length us, event | category | flops | bytes accessed | tf_op | source)
XLA Modules:
  0.0 57.5 jit_solution(5945061701835944487)
XLA Ops:
  0.6 55.5 %shard_map.203 = (bf16[32,2048]{1,0:T(8,128)(2,1)S(1)}, bf16[128,512]{1,0:T(8,128)(2,1)S(1)}) custom-call(bf16[128,512]{1,0:T(8,128)(2,1)} %refs_0_.1, f32[512]{0:T(512)} %refs_1_.1, bf16[32,128]{1,0:T(8,128)(2,1)} %bitcast.3, f32[32,1024]{1,0:T(8,128)} %constant.2.clone.refs_3_, s32[4,128]{1,0:T(4,128)} %bitcast.4, f32[4,128]{1,0:T(4,128)} %bitcast.5, ...), custom_call_target="tpu_custom_call" | custom-call | tf_op jit(solution)/shard_map/pallas_call | solution.py:845
  56.1 0.7 %copy.24 = bf16[32,2048]{1,0:T(8,128)(2,1)} copy(bf16[32,2048]{1,0:T(8,128)(2,1)S(1)} %get-tuple-element.2) | data formatting | bytes 262144
  56.8 0.7 %copy.25 = bf16[128,512]{1,0:T(8,128)(2,1)} copy(bf16[128,512]{1,0:T(8,128)(2,1)S(1)} %get-tuple-element.3) | data formatting | bytes 262144

commit v2 on v1

--- a/solution.py
+++ b/solution.py
@@ -260,47 +260,66 @@
 QUERY, PROJECT, ATTEND, HEAD_OUT, MIX_SEND, MIX_DONE = range(10, 16)
 EXPERTS, FAR, SIDE_X, SIDE_Y, OWN = range(16, 21)
 SCHEDULE = (
-    (LAT, C, 0, 0), (TOK, A, 1, 0), (LAT, A, 1, 0), (TOK, A, 2, 0), (TOK, C, 0, 1),
-    (TOK, B, 1, 0), (TOK, A, 1, 1), (LAT, A, 2, 0), (TOK, B, 2, 0), (TOK, A, 2, 1),
-    (TOK, C, 0, 0), (TOK, B, 1, 1), (TOK, C, 2, 0), (TOK, KC, 0, 0), (EXPERTS, 0, 0),
-    (LAT, B, 1, 0), (LAT, C, 2, 0), (TOK, C, 1, 1), (TOK, D, 0, 0), (TOK, D, 0, 1),
-    (TOK, C, 2, 1), (TOK, A, 3, 0), (TOK, D, 2, 0), (TOK, D, 1, 1), (LAT, A, 3, 0),
-    (LAT, B, 2, 0), (LAT, D, 0, 0), (LAT, KC, 2, 0), (TOK, A, 3, 1), (LAT, C, 1, 0),
-    (TOK, KD, 2, 0), (LAT, D, 1, 0), (LAT, D, 2, 0), (LAT, KC, 1, 0), (TOK, B, 2, 1),
-    (TOK, D, 2, 1), (TOK, KC, 0, 1), (TOK, KB, 2, 0), (LAT, KD, 2, 0), (TOK, KA, 2, 1), (QUERY,),
-    (TOK, KB, 2, 1), (TOK, C, 1, 0), (TOK, KA, 2, 0), (TOK, C, 3, 0), (LAT, KD, 0, 0),
-    (LAT, KA, 2, 0), (LAT, KB, 2, 0), (TOK, KC, 2, 0), (TOK, KA, 1, 0), (LAT, KB, 1, 0),
-    (TOK, KD, 0, 1), (TOK, KC, 1, 1), (LAT, KD, 1, 0), (TOK, B, 3, 0), (TOK, D, 1, 0),
-    (TOK, KA, 3, 1), (TOK, KC, 2, 1), (TOK, KD, 1, 1), (TOK, KD, 2, 1), (LAT, C, 3, 0),
-    (EXPERTS, 2, 1), (TOK, C, 3, 1), (EXPERTS, 2, 0), (LAT, KC, 3, 0), (TOK, KC, 1, 0),
-    (LAT, B, 3, 0), (FAR, 2), (TOK, KD, 1, 0), (TOK, B, 3, 1), (TOK, KD, 0, 0), (EXPERTS, 1, 1),
-    (LAT, KC, 0, 0), (TOK, KC, 3, 1), (FAR, 1), (LAT, D, 3, 0), (TOK, KA, 3, 0), (LAT, KB, 3, 0),
-    (TOK, KA, 1, 1), (TOK, D, 3, 1), (TOK, D, 3, 0), (EXPERTS, 0, 1), (TOK, KC, 3, 0),
-    (LAT, KA, 3, 0), (SIDE_X, 2), (TOK, KB, 1, 1), (SIDE_Y, 2), (TOK, KD, 3, 0), (TOK, KB, 1, 0),
-    (LAT, KA, 1, 0), (EXPERTS, 1, 0), (LAT, KD, 3, 0), (TOK, KD, 3, 1), (TOK, KB, 3, 0),
-    (EXPERTS, 3, 1), (FAR, 0), (TOK, KB, 3, 1), (PROJECT,), (ATTEND, 3), (FAR, 3), (SIDE_X, 1),
-    (SIDE_Y, 1), (OWN, 2), (EXPERTS, 3, 0), (SIDE_X, 3), (SIDE_Y, 3), (SIDE_Y, 0), (SIDE_X, 0),
-    (ATTEND, 0), (ATTEND, 2), (OWN, 1), (ATTEND, 1), (HEAD_OUT,), (OWN, 3), (MIX_SEND,), (OWN, 0),
+    (LAT, A, 1, 0), (LAT, A, 2, 0), (TOK, A, 1, 0), (TOK, A, 2, 0), (LAT, C, 0, 0),
+    (EXPERTS, 0, 0), (TOK, A, 1, 1), (TOK, KA, 1, 0), (TOK, A, 2, 1), (TOK, C, 0, 0),
+    (TOK, C, 0, 1), (LAT, C, 2, 0), (TOK, B, 2, 0), (LAT, B, 2, 0), (TOK, B, 1, 0),
+    (TOK, C, 2, 1), (TOK, A, 3, 1), (TOK, D, 0, 1), (TOK, C, 2, 0), (TOK, KC, 2, 1),
+    (LAT, C, 1, 0), (QUERY,), (TOK, D, 2, 0), (TOK, B, 1, 1), (TOK, A, 3, 0), (LAT, D, 2, 0),
+    (TOK, KA, 3, 1), (LAT, A, 3, 0), (TOK, C, 1, 0), (TOK, B, 2, 1), (TOK, KC, 2, 0),
+    (LAT, KD, 2, 0), (TOK, KB, 1, 0), (TOK, D, 2, 1), (TOK, KC, 1, 0), (LAT, KA, 2, 0),
+    (LAT, KC, 2, 0), (TOK, D, 1, 0), (TOK, C, 1, 1), (LAT, KC, 0, 0), (LAT, B, 1, 0),
+    (TOK, KC, 0, 0), (TOK, KB, 1, 1), (TOK, KD, 2, 1), (TOK, KC, 0, 1), (TOK, KD, 2, 0),
+    (EXPERTS, 2, 1), (LAT, D, 0, 0), (LAT, KA, 1, 0), (TOK, C, 3, 1), (TOK, KB, 2, 1),
+    (LAT, KB, 2, 0), (LAT, D, 1, 0), (TOK, KA, 2, 0), (TOK, KC, 1, 1), (TOK, D, 1, 1),
+    (TOK, D, 0, 0), (FAR, 2), (TOK, B, 3, 0), (LAT, KD, 1, 0), (TOK, KD, 0, 1), (TOK, KD, 1, 0),
+    (LAT, KD, 0, 0), (LAT, KC, 1, 0), (TOK, KD, 1, 1), (EXPERTS, 1, 1), (LAT, C, 3, 0),
+    (TOK, KA, 3, 0), (TOK, KD, 0, 0), (TOK, KB, 2, 0), (TOK, KA, 1, 1), (TOK, B, 3, 1),
+    (LAT, B, 3, 0), (TOK, KA, 2, 1), (EXPERTS, 2, 0), (TOK, C, 3, 0), (FAR, 1), (TOK, D, 3, 1),
+    (LAT, KA, 3, 0), (EXPERTS, 0, 1), (SIDE_Y, 2), (SIDE_X, 2), (LAT, KC, 3, 0), (LAT, KB, 1, 0),
+    (TOK, KD, 3, 1), (LAT, D, 3, 0), (TOK, D, 3, 0), (FAR, 0), (LAT, KB, 3, 0), (TOK, KC, 3, 1),
+    (TOK, KB, 3, 1), (EXPERTS, 1, 0), (TOK, KC, 3, 0), (TOK, KD, 3, 0), (LAT, KD, 3, 0),
+    (TOK, KB, 3, 0), (EXPERTS, 3, 1), (EXPERTS, 3, 0), (FAR, 3), (SIDE_X, 1), (OWN, 2),
+    (SIDE_Y, 1), (PROJECT,), (ATTEND, 3), (ATTEND, 2), (SIDE_Y, 3), (SIDE_Y, 0), (SIDE_X, 3),
+    (ATTEND, 1), (OWN, 1), (SIDE_X, 0), (ATTEND, 0), (HEAD_OUT,), (OWN, 3), (MIX_SEND,), (OWN, 0),
     (MIX_DONE,),
 )
-OVER_Y = ((0, 1, 0), (1, 0, 0), (1, 1, 0), (1, 1, 1), (1, 3, 0),)
+OVER_Y = ((0, 0, 0), (0, 2, 0), (1, 0, 1), (1, 1, 0), (1, 1, 1), (1, 2, 0), (1, 3, 0),)
 CHUNKS = (1, 2)
-B_OVER_Z = (False, True)
-C_OVER_Z = (False, True)
+B_OVER_Z = (False, False)
+C_OVER_Z = (True, True)
 LAST_TURN = max(entry[2] for entry in SCHEDULE if entry[0] in (LAT, TOK))
 
 
 def relay_way(which, turn, chunk):
     return "y" if (which, turn, chunk) in OVER_Y else "x"
+
+
+def over_line(which, name, turn):
+    return turn and (
+        name == A or turn == 1 and (name == B and B_OVER_Z[which] or name == C and C_OVER_Z[which])
+    )
 
 
 def gather_keys(dims):
     keys = []
     for which in range(2):
         for turn in range(dims[0]):
-            names = ["C", "D", "kC", "kD"]
-            names += ["F", "B", "kA", "kB"] if turn else ["L", "R", "BL", "BR", "CL", "CR"]
-            keys += [(which, n, turn, c) for n in names for c in range(CHUNKS[which])]
+            names = [C, D, KC, KD] + ([A, B, KA, KB] if turn else [])
+            keys += [
+                (which, name, turn, chunk)
+                for name in names
+                if not over_line(which, name, turn)
+                for chunk in range(CHUNKS[which])
+            ]
+    return {key: index for index, key in enumerate(keys)}
+
+
+def line_keys(dims):
+    keys = []
+    for which in range(2):
+        for chunk in range(CHUNKS[which]):
+            keys += [(which, A, place, chunk) for place in range(dims[0])]
+            keys += [(which, name, 1, chunk) for name in (B, C) if over_line(which, name, 1)]
     return {key: index for index, key in enumerate(keys)}
 
 
@@ -323,27 +342,16 @@
 
 
 LOADS = (
-    "kl",
-    "kg",
-    "rk",
-    "tab",
-    "rid",
-    "rwt",
-    "sr",
-    "sg",
-    "ql",
-    "qg",
-    "qw",
-    "gate",
-    "up",
-    "shg",
-    "shu",
-    "down",
-    "shd",
-    "kw",
-    "ow",
-    "og",
+    ("kl", "kg", "rk", "tab", "rid", "rwt"),
+    ("sr", "sg"),
+    ("ql", "qg", "qw"),
+    ("gate", "up"),
+    ("shg", "shu", "down", "shd"),
+    ("kw",),
+    ("ow",),
+    ("og",),
 )
+LOADED = [name for group in LOADS for name in group]
 
 
 def layer_kernel(dims, names, *refs):
@@ -352,7 +360,7 @@
     me = place_of(dims)
     ep_at = lax.axis_index("ep")
     ep_count = dims[0] * dims[1]
-    g_keys, r_keys = gather_keys(dims), reduce_keys(dims)
+    g_keys, l_keys, r_keys = gather_keys(dims), line_keys(dims), reduce_keys(dims)
     slots, _ = reduce_slots(dims)
     zs = line_order(me[0], z_count)
     lat, tok = ref["lat_all"], ref["tok_all"]
@@ -366,7 +374,8 @@
     sent = []
 
     local = {}
-    for number, name in enumerate(LOADS):
+    number_of = {name: number for number, group in enumerate(LOADS) for name in group}
+    for name in LOADED:
         source, target = ref["h_" + name], ref["v_" + name] if "v_" + name in ref else None
         if name == "tab":
             source = source.at[:, own_rows]
@@ -378,7 +387,7 @@
         elif name in ("shg", "shu"):
             width = source.shape[1]
             target = ref["v_sgu"].at[:, pl.ds(width * (name == "shu"), width)]
-        local[name] = pltpu.make_async_copy(source, target, ref["load_sem"].at[number])
+        local[name] = pltpu.make_async_copy(source, target, ref["load_sem"].at[number_of[name]])
         local[name].start()
 
     def loaded(*wanted):
@@ -386,14 +395,27 @@
             local[name].wait()
 
     barrier = pltpu.get_barrier_semaphore()
-    peers = [{"dz": dz} for dz in range(1, z_count)] + [{"dy": 1}, {"dx": 1}, {"dk": 1}]
-    for peer in peers:
+    for there, target in ((me[0] > 0, me[0] - 1), (me[0] + 1 < z_count, me[0] + 1)):
+        neighbour = (jnp.where(there, target, me[0]),) + me[1:]
+
+        @pl.when(there)
+        def _():
+            pl.semaphore_signal(
+                barrier,
+                inc=1,
+                device_id=device_of(dims, neighbour),
+                device_id_type=MESH,
+            )
+
+    sides = ({"dy": 1}, {"dx": 1}, {"dk": 1})
+    for side in sides:
         pl.semaphore_signal(
             barrier,
             inc=1,
-            device_id=device_of(dims, moved(dims, me, **peer)),
+            device_id=device_of(dims, moved(dims, me, **side)),
             device_id_type=MESH,
         )
+    met = len(sides) + jnp.where(me[0] > 0, 1, 0) + jnp.where(me[0] + 1 < z_count, 1, 0)
 
     def at_place(turn, dy=0, dx=0, dk=0):
         return (zs[turn],) + moved(dims, me, dy=dy, dx=dx, dk=dk)[1:]
@@ -413,7 +435,7 @@
         return pltpu.make_async_remote_copy(
             src_ref=at,
             dst_ref=at,
-            send_sem=ref["g_send"].at[g_keys[key]],
+            send_sem=ref["send"].at[0],
             recv_sem=ref["g_recv"].at[g_keys[key]],
             device_id=device_of(dims, target),
             device_id_type=MESH,
@@ -424,14 +446,18 @@
         copy.start()
         sent.append(copy)
 
-    def line_copy(which, key, place, chunk, target_z):
+    def line_copy(key, place, target_z):
+        which, name, _, chunk = key
         at = region(which, place, chunk)
-        kind = "BC".find(key[1][0]) + 1
+        if name == A:
+            number = l_keys[(which, A, 0, chunk)] + place[0]
+        else:
+            number = l_keys[key]
         return pltpu.make_async_remote_copy(
             src_ref=at,
             dst_ref=at,
-            send_sem=ref["g_send"].at[g_keys[key]],
-            recv_sem=ref["line_recv"].at[which * 3 + kind, place[0], chunk],
+            send_sem=ref["send"].at[0],
+            recv_sem=ref["line_recv"].at[number],
             device_id=device_of(dims, (target_z,) + me[1:]),
             device_id_type=MESH,
         )
@@ -441,9 +467,9 @@
     def line_send(key, place, down):
         target = jnp.where(down, me[0] - 1, me[0] + 1)
         there = (target >= 0) & (target < z_count)
-        if key[1][0] in "BC":
+        if key[1] != A:
             there &= line_order(target, z_count)[1] == me[0]
-        copy = line_copy(key[0], key, place, key[3], jnp.where(there, target, me[0]))
+        copy = line_copy(key, place, jnp.where(there, target, me[0]))
 
         @pl.when(there)
         def _():
@@ -451,23 +477,25 @@
 
         line_sent.append((there, copy))
 
+    def both_ways(key, place):
+        line_send(key, place, True)
+        line_send(key, place, False)
+
     def take(which, name, turn, chunk):
         place = place_from(name, turn)
-        if name == "A":
-            key = (which, "F", turn, chunk)
-            line_copy(which, key, place, chunk, me[0]).wait_recv()
+        key = (which, name, turn, chunk)
+        if over_line(which, name, turn):
+            line_copy(key, place, me[0]).wait_recv()
+        else:
+            g_copy(key, place, me).wait_recv()
+        if name == A:
             line_send(key, place, place[0] > me[0])
-            if not (turn == 1 and B_OVER_Z[which]):
-                g_send((which, "B", turn, chunk), place, dx=1)
-            if not (turn == 1 and C_OVER_Z[which]):
-                g_send((which, "C", turn, chunk), place, dy=1)
-        elif turn == 1 and (name == "B" and B_OVER_Z[which] or name == "C" and C_OVER_Z[which]):
-            line_copy(which, (which, name + "L", 0, chunk), place, chunk, me[0]).wait_recv()
-        else:
-            g_copy((which, name, turn, chunk), place, me).wait_recv()
-        if name == "C" and turn == 0 and C_OVER_Z[which]:
-            line_send((which, "CL", 0, chunk), place, True)
-            line_send((which, "CR", 0, chunk), place, False)
+            if not over_line(which, B, turn):
+                g_send((which, B, turn, chunk), place, dx=1)
+            if not over_line(which, C, turn):
+                g_send((which, C, turn, chunk), place, dy=1)
+        if name == C and turn == 0 and over_line(which, C, 1):
+            both_ways((which, C, 1, chunk), place)
         way = relay_way(which, turn, chunk)
         if name == "B" and turn and way == "y":
             g_send((which, "D", turn, chunk), place, dy=1)
@@ -508,21 +536,20 @@
     )
     lat[own_rows, tile_at] = upright.T.astype(jnp.bfloat16)
 
-    pl.semaphore_wait(barrier, len(peers))
+    pl.semaphore_wait(barrier, met)
 
     def send_own(which):
         for chunk in range(CHUNKS[which]):
-            line_send((which, "L", 0, chunk), me, True)
-            line_send((which, "R", 0, chunk), me, False)
-            g_send((which, "C", 0, chunk), me, dy=1)
+            both_ways((which, A, 0, chunk), me)
+            g_send((which, C, 0, chunk), me, dy=1)
 
     def send_mirror(which):
+        mirror = at_place(0, 0, 1)
         for chunk in range(CHUNKS[which]):
             if relay_way(which, 0, chunk) == "y":
-                g_send((which, "D", 0, chunk), at_place(0, 0, 1), dy=1)
-            if B_OVER_Z[which]:
-                line_send((which, "BL", 0, chunk), at_place(0, 0, 1), True)
-                line_send((which, "BR", 0, chunk), at_place(0, 0, 1), False)
+                g_send((which, D, 0, chunk), mirror, dy=1)
+            if over_line(which, B, 1):
+                both_ways((which, B, 1, chunk), mirror)
 
     send_own(0)
     send_mirror(0)
@@ -603,7 +630,7 @@
         return pltpu.make_async_remote_copy(
             src_ref=source,
             dst_ref=stores[group].at[index],
-            send_sem=ref["r_send"].at[r_keys[key]],
+            send_sem=ref["send"].at[0],
             recv_sem=ref["r_recv"].at[r_keys[key]],
             device_id=device_of(dims, target),
             device_id_type=MESH,
@@ -719,7 +746,7 @@
         return pltpu.make_async_remote_copy(
             src_ref=source,
             dst_ref=ref["line_parts"].at[slot],
-            send_sem=ref["line_send"].at[slot],
+            send_sem=ref["send"].at[0],
             recv_sem=ref["line_done"].at[slot],
             device_id=device_of(dims, (target_z,) + me[1:]),
             device_id_type=MESH,
@@ -805,7 +832,7 @@
     bf16 = jnp.bfloat16
     scratch = {
         "v_" + name: pltpu.VMEM(given[name].shape, given[name].dtype)
-        for name in LOADS
+        for name in LOADED
         if name not in ("tab", "gate", "up", "down", "shg", "shu")
     }
     hidden = gate.shape[2]
@@ -831,16 +858,14 @@
         "sums": pltpu.VMEM((dims[0] * 4, rows, width), bf16),
         "mix_sum": pltpu.VMEM((mix_rows, model_width), bf16),
         "line_parts": pltpu.VMEM((dims[0], rows, width), bf16),
-        "line_send": pltpu.SemaphoreType.DMA((dims[0],)),
         "line_done": pltpu.SemaphoreType.DMA((dims[0],)),
-        "line_recv": pltpu.SemaphoreType.DMA((6, dims[0], max(CHUNKS))),
+        "line_recv": pltpu.SemaphoreType.DMA((len(line_keys(dims)),)),
         "load_sem": pltpu.SemaphoreType.DMA((len(LOADS),)),
-        "g_send": pltpu.SemaphoreType.DMA((len(gather_keys(dims)),)),
+        "send": pltpu.SemaphoreType.DMA((1,)),
         "g_recv": pltpu.SemaphoreType.DMA((len(gather_keys(dims)),)),
-        "r_send": pltpu.SemaphoreType.DMA((len(reduce_keys(dims)),)),
         "r_recv": pltpu.SemaphoreType.DMA((len(reduce_keys(dims)),)),
     }
-    names = ["h_" + name for name in LOADS] + ["mixed", "out"] + list(scratch)
+    names = ["h_" + name for name in LOADED] + ["mixed", "out"] + list(scratch)
     vmem = pl.BlockSpec(memory_space=pltpu.VMEM)
     return pl.pallas_call(
         functools.partial(layer_kernel, dims, names),
@@ -848,13 +873,13 @@
             pltpu.VMEM((mix_rows, model_width), bf16),
             pltpu.VMEM((rows, width), bf16),
         ],
-        in_specs=[pl.BlockSpec(memory_space=pltpu.HBM)] * len(LOADS),
+        in_specs=[pl.BlockSpec(memory_space=pltpu.HBM)] * len(LOADED),
         out_specs=[vmem] * 2,
         scratch_shapes=list(scratch.values()),
         compiler_params=pltpu.CompilerParams(
             collective_id=0, has_side_effects=True, vmem_limit_bytes=56 * 1024 * 1024
         ),
-    )(*[given[name] for name in LOADS])
+    )(*[given[name] for name in LOADED])
 
 
 def solution(mesh):

time: 57.6 us -> 52.6 us (0.913)
  Pallas kernels: 55.5 us -> 50.5 us
    pallas_call x1, Pallas kernels: 55.5 us -> 50.5 us  [per_device_fused(): pl.pallas_call(functools.partial(layer_kernel, dims, names), out_shape=[p...]
where the time goes in v2:
time: 52.6 us; the launch traced here: 52.5 us
  Pallas kernels  50.5 us (96%)
  local copies, waits for them, and re-layouts  1.31 us (2%)
  between operations  0.65 us (1%)
    pallas_call x1, Pallas kernels, per_device_fused(): pl.pallas_call(functools.partial(layer_kernel, dims, names), out_shape=[p...  50.5 us
    unnamed x2, local copies, waits for them, and re-layouts  1.31 us

profile of v2, /device:TPU:0, one launch (start us, length us, event | category | flops | bytes accessed | tf_op | source)
XLA Modules:
  0.0 52.5 jit_solution(123482429755979933)
XLA Ops:
  0.6 50.5 %shard_map.203 = (bf16[32,2048]{1,0:T(8,128)(2,1)S(1)}, bf16[128,512]{1,0:T(8,128)(2,1)S(1)}) custom-call(bf16[128,512]{1,0:T(8,128)(2,1)} %refs_0_.1, f32[512]{0:T(512)} %refs_1_.1, bf16[32,128]{1,0:T(8,128)(2,1)} %bitcast.3, f32[32,1024]{1,0:T(8,128)} %constant.2.clone.refs_3_, s32[4,128]{1,0:T(4,128)} %bitcast.4, f32[4,128]{1,0:T(4,128)} %bitcast.5, ...), custom_call_target="tpu_custom_call" | custom-call | tf_op jit(solution)/shard_map/pallas_call | solution.py:870
  51.1 0.7 %copy.24 = bf16[32,2048]{1,0:T(8,128)(2,1)} copy(bf16[32,2048]{1,0:T(8,128)(2,1)S(1)} %get-tuple-element.2) | data formatting | bytes 262144
  51.8 0.7 %copy.25 = bf16[128,512]{1,0:T(8,128)(2,1)} copy(bf16[128,512]{1,0:T(8,128)(2,1)S(1)} %get-tuple-element.3) | data formatting | bytes 262144

commit v3 on v2

--- a/solution.py
+++ b/solution.py
@@ -256,37 +256,31 @@
 
 LAT, TOK = 0, 1
 A, B, C, D = "A", "B", "C", "D"
-KA, KB, KC, KD = "kA", "kB", "kC", "kD"
 QUERY, PROJECT, ATTEND, HEAD_OUT, MIX_SEND, MIX_DONE = range(10, 16)
 EXPERTS, FAR, SIDE_X, SIDE_Y, OWN = range(16, 21)
 SCHEDULE = (
-    (LAT, A, 1, 0), (LAT, A, 2, 0), (TOK, A, 1, 0), (TOK, A, 2, 0), (LAT, C, 0, 0),
-    (EXPERTS, 0, 0), (TOK, A, 1, 1), (TOK, KA, 1, 0), (TOK, A, 2, 1), (TOK, C, 0, 0),
-    (TOK, C, 0, 1), (LAT, C, 2, 0), (TOK, B, 2, 0), (LAT, B, 2, 0), (TOK, B, 1, 0),
-    (TOK, C, 2, 1), (TOK, A, 3, 1), (TOK, D, 0, 1), (TOK, C, 2, 0), (TOK, KC, 2, 1),
-    (LAT, C, 1, 0), (QUERY,), (TOK, D, 2, 0), (TOK, B, 1, 1), (TOK, A, 3, 0), (LAT, D, 2, 0),
-    (TOK, KA, 3, 1), (LAT, A, 3, 0), (TOK, C, 1, 0), (TOK, B, 2, 1), (TOK, KC, 2, 0),
-    (LAT, KD, 2, 0), (TOK, KB, 1, 0), (TOK, D, 2, 1), (TOK, KC, 1, 0), (LAT, KA, 2, 0),
-    (LAT, KC, 2, 0), (TOK, D, 1, 0), (TOK, C, 1, 1), (LAT, KC, 0, 0), (LAT, B, 1, 0),
-    (TOK, KC, 0, 0), (TOK, KB, 1, 1), (TOK, KD, 2, 1), (TOK, KC, 0, 1), (TOK, KD, 2, 0),
-    (EXPERTS, 2, 1), (LAT, D, 0, 0), (LAT, KA, 1, 0), (TOK, C, 3, 1), (TOK, KB, 2, 1),
-    (LAT, KB, 2, 0), (LAT, D, 1, 0), (TOK, KA, 2, 0), (TOK, KC, 1, 1), (TOK, D, 1, 1),
-    (TOK, D, 0, 0), (FAR, 2), (TOK, B, 3, 0), (LAT, KD, 1, 0), (TOK, KD, 0, 1), (TOK, KD, 1, 0),
-    (LAT, KD, 0, 0), (LAT, KC, 1, 0), (TOK, KD, 1, 1), (EXPERTS, 1, 1), (LAT, C, 3, 0),
-    (TOK, KA, 3, 0), (TOK, KD, 0, 0), (TOK, KB, 2, 0), (TOK, KA, 1, 1), (TOK, B, 3, 1),
-    (LAT, B, 3, 0), (TOK, KA, 2, 1), (EXPERTS, 2, 0), (TOK, C, 3, 0), (FAR, 1), (TOK, D, 3, 1),
-    (LAT, KA, 3, 0), (EXPERTS, 0, 1), (SIDE_Y, 2), (SIDE_X, 2), (LAT, KC, 3, 0), (LAT, KB, 1, 0),
-    (TOK, KD, 3, 1), (LAT, D, 3, 0), (TOK, D, 3, 0), (FAR, 0), (LAT, KB, 3, 0), (TOK, KC, 3, 1),
-    (TOK, KB, 3, 1), (EXPERTS, 1, 0), (TOK, KC, 3, 0), (TOK, KD, 3, 0), (LAT, KD, 3, 0),
-    (TOK, KB, 3, 0), (EXPERTS, 3, 1), (EXPERTS, 3, 0), (FAR, 3), (SIDE_X, 1), (OWN, 2),
-    (SIDE_Y, 1), (PROJECT,), (ATTEND, 3), (ATTEND, 2), (SIDE_Y, 3), (SIDE_Y, 0), (SIDE_X, 3),
-    (ATTEND, 1), (OWN, 1), (SIDE_X, 0), (ATTEND, 0), (HEAD_OUT,), (OWN, 3), (MIX_SEND,), (OWN, 0),
-    (MIX_DONE,),
+    (LAT, A, 1, 0), (LAT, C, 0, 0), (TOK, A, 1, 0), (LAT, A, 2, 0), (TOK, A, 2, 0),
+    (TOK, A, 1, 1), (TOK, A, 2, 1), (LAT, A, 3, 0), (TOK, C, 0, 1), (LAT, D, 0, 0),
+    (LAT, B, 1, 0), (EXPERTS, 0, 0), (LAT, C, 2, 0), (TOK, C, 0, 0), (TOK, B, 2, 0),
+    (LAT, B, 2, 0), (TOK, B, 1, 1), (TOK, C, 2, 1), (TOK, B, 1, 0), (TOK, A, 3, 1),
+    (TOK, B, 2, 1), (TOK, C, 2, 0), (TOK, A, 3, 0), (TOK, C, 1, 1), (TOK, D, 2, 0),
+    (LAT, D, 2, 0), (TOK, D, 2, 1), (EXPERTS, 2, 0), (LAT, C, 1, 0), (TOK, D, 0, 0),
+    (EXPERTS, 2, 1), (TOK, D, 1, 1), (LAT, C, 3, 0), (EXPERTS, 1, 0), (TOK, D, 0, 1),
+    (TOK, B, 3, 0), (FAR, 2), (TOK, C, 1, 0), (TOK, B, 3, 1), (QUERY,), (LAT, D, 1, 0),
+    (TOK, C, 3, 1), (LAT, B, 3, 0), (SIDE_X, 1, 1), (TOK, D, 1, 0), (LAT, D, 3, 0),
+    (EXPERTS, 1, 1), (PROJECT,), (SIDE_X, 2, 1), (SIDE_Y, 2, 1), (TOK, C, 3, 0), (ATTEND, 2),
+    (FAR, 1), (TOK, D, 3, 0), (TOK, D, 3, 1), (SIDE_Y, 1, 0), (EXPERTS, 0, 1), (SIDE_X, 2, 0),
+    (SIDE_Y, 2, 0), (EXPERTS, 3, 1), (SIDE_X, 0, 1), (OWN, 2, 1), (FAR, 3), (SIDE_Y, 1, 1),
+    (ATTEND, 0), (SIDE_X, 1, 0), (ATTEND, 1), (EXPERTS, 3, 0), (FAR, 0), (ATTEND, 3), (HEAD_OUT,),
+    (SIDE_Y, 3, 0), (OWN, 2, 0), (OWN, 1, 1), (SIDE_X, 3, 0), (OWN, 1, 0), (SIDE_X, 3, 1),
+    (SIDE_Y, 3, 1), (MIX_SEND,), (OWN, 3, 0), (SIDE_Y, 0, 1), (OWN, 3, 1), (SIDE_X, 0, 0),
+    (SIDE_Y, 0, 0), (MIX_DONE,), (OWN, 0, 1), (OWN, 0, 0),
 )
-OVER_Y = ((0, 0, 0), (0, 2, 0), (1, 0, 1), (1, 1, 0), (1, 1, 1), (1, 2, 0), (1, 3, 0),)
+OVER_Y = ((0, 2, 0), (1, 0, 0), (1, 0, 1), (1, 1, 0), (1, 1, 1), (1, 2, 0), (1, 3, 0),)
 CHUNKS = (1, 2)
 B_OVER_Z = (False, False)
 C_OVER_Z = (True, True)
+SIDE_OVER_Z = (True, True)
 LAST_TURN = max(entry[2] for entry in SCHEDULE if entry[0] in (LAT, TOK))
 
 
@@ -304,7 +298,7 @@
     keys = []
     for which in range(2):
         for turn in range(dims[0]):
-            names = [C, D, KC, KD] + ([A, B, KA, KB] if turn else [])
+            names = [C, D] + ([A, B] if turn else [])
             keys += [
                 (which, name, turn, chunk)
                 for name in names
@@ -314,6 +308,17 @@
     return {key: index for index, key in enumerate(keys)}
 
 
+def pair_keys(dims):
+    keys = [
+        (which, name, turn, chunk)
+        for which in range(2)
+        for turn in range(dims[0])
+        for name in ((A, B, C, D) if turn else (C, D))
+        for chunk in range(CHUNKS[which])
+    ]
+    return {key: index for index, key in enumerate(keys)}
+
+
 def line_keys(dims):
     keys = []
     for which in range(2):
@@ -327,7 +332,8 @@
     keys = []
     for turn in range(dims[0]):
         keys += [("k", turn, dy, dx) for dy in range(2) for dx in range(2)]
-        keys += [("p", turn), ("q", turn), ("x", turn), ("y", turn)]
+        keys += [("p", turn), ("q", turn)]
+        keys += [(side, turn, half) for side in ("x", "y") for half in range(2)]
     keys += [("mk", 0), ("mk", 1), ("mx", 0)]
     return {key: index for index, key in enumerate(keys)}
 
@@ -335,7 +341,7 @@
 def reduce_slots(dims):
     slots, sizes = {}, {"half": 0, "mix": 0, "full": 0}
     for key in reduce_keys(dims):
-        group = "half" if key[0] in "pq" else ("mix" if key[0][0] == "m" else "full")
+        group = "full" if key[0] == "k" else ("mix" if key[0][0] == "m" else "half")
         slots[key] = (group, sizes[group])
         sizes[group] += 1
     return slots, sizes
@@ -360,6 +366,7 @@
     me = place_of(dims)
     ep_at = lax.axis_index("ep")
     ep_count = dims[0] * dims[1]
+    p_keys = pair_keys(dims)
     g_keys, l_keys, r_keys = gather_keys(dims), line_keys(dims), reduce_keys(dims)
     slots, _ = reduce_slots(dims)
     zs = line_order(me[0], z_count)
@@ -426,9 +433,7 @@
         return alls[which].at[pl.ds(begin, size), :]
 
     def place_from(name, turn):
-        return at_place(turn, *{"A": (0, 0), "B": (0, 1), "C": (1, 0), "D": (1, 1)}[name[-1]])[
-            :3
-        ] + ((moved(dims, me, dk=1) if name[0] == "k" else me)[3],)
+        return at_place(turn, int(name in (C, D)), int(name in (B, D)))
 
     def g_copy(key, place, target):
         at = region(key[0], place, key[3])
@@ -440,6 +445,30 @@
             device_id=device_of(dims, target),
             device_id_type=MESH,
         )
+
+    def pair_copy(key, place, target):
+        which, name, turn, chunk = key
+        at = region(which, place, chunk)
+        return pltpu.make_async_remote_copy(
+            src_ref=at,
+            dst_ref=at,
+            send_sem=ref["send"].at[0],
+            recv_sem=ref["pair_recv"].at[p_keys[key]],
+            device_id=device_of(dims, target),
+            device_id_type=MESH,
+        )
+
+    paired = set()
+
+    def pair(which, turn, dy):
+        if (which, turn, dy) in paired or not (turn or dy):
+            return
+        paired.add((which, turn, dy))
+        for name in (C, D) if dy else (A, B):
+            place = place_from(name, turn)
+            other = place[:3] + (moved(dims, me, dk=1)[3],)
+            for chunk in range(CHUNKS[which]):
+                pair_copy((which, name, turn, chunk), other, me).wait_recv()
 
     def g_send(key, place, **step):
         copy = g_copy(key, place, moved(dims, me, **step))
@@ -457,7 +486,7 @@
             src_ref=at,
             dst_ref=at,
             send_sem=ref["send"].at[0],
-            recv_sem=ref["line_recv"].at[number],
+            recv_sem=ref["lr"].at[number],
             device_id=device_of(dims, (target_z,) + me[1:]),
             device_id_type=MESH,
         )
@@ -501,8 +530,9 @@
             g_send((which, "D", turn, chunk), place, dy=1)
         if name == "C" and way == "x":
             g_send((which, "D", turn, chunk), place, dx=1)
-        if name[0] != "k":
-            g_send((which, "k" + name, turn, chunk), place, dk=1)
+        copy = pair_copy(key, place, moved(dims, me, dk=1))
+        copy.start()
+        sent.append(copy)
 
     def rms(values, gain):
         widened = values.astype(jnp.float32)
@@ -598,6 +628,9 @@
 
     def project():
         loaded("kw")
+        for turn in range(z_count):
+            pair(LAT, turn, 0)
+            pair(LAT, turn, 1)
         ref["kv_all"][...] = jnp.dot(
             lat[:, pl.ds(0, latent_width)], ref["v_kw"][...], preferred_element_type=jnp.float32
         ).astype(jnp.bfloat16)
@@ -686,6 +719,8 @@
         return gate_act / (1.0 + jnp.exp(-gate_act)) * up_act
 
     def experts(dz, dy):
+        pair(LAT, dz, dy)
+        pair(TOK, dz, dy)
         begin = device_of(dims, at_place(dz, dy))[0] * rows
         span = pl.ds(pl.multiple_of(begin, rows), rows)
         tokens = tok[span, :]
@@ -715,58 +750,111 @@
         for dx in (1, 0):
             r_send(("k", dz, dy, dx), part_of(dz, dy, dx, 1), dk=1)
 
-    def core_sum(dz, dy, dx):
-        return part_of(dz, dy, dx, 0)[...].astype(jnp.float32) + landed(("k", dz, dy, dx))
-
-    def keep(dz, dy, dx, value):
-        index = dz * 4 + dy * 2 + dx
-        sums[index] = value.astype(jnp.bfloat16)
-        return sums.at[index]
-
     half_rows = rows // 2
+    both_cores = set()
+
+    def core_sum(dz, dy, dx, half):
+        key = ("k", dz, dy, dx)
+        at = stores["full"].at[slots[key][1]]
+        if key not in both_cores:
+            both_cores.add(key)
+            r_copy(key, at, me).wait_recv()
+        span = pl.ds(half * half_rows, half_rows)
+        mine = part_of(dz, dy, dx, 0)[span, :].astype(jnp.float32)
+        return mine + at[span, :].astype(jnp.float32)
+
+    def keep(dz, dy, dx, half, value):
+        at = sums.at[dz * 4 + dy * 2 + dx, pl.ds(half * half_rows, half_rows)]
+        at[...] = value.astype(jnp.bfloat16)
+        return at
 
     def finish_far(dz):
-        at = keep(dz, 1, 1, core_sum(dz, 1, 1))
-        r_send(("p", dz), at.at[pl.ds(0, half_rows)], dy=1)
-        r_send(("q", dz), at.at[pl.ds(half_rows, half_rows)], dx=1)
-
-    def finish_side_y(dz):
-        value = core_sum(dz, 1, 0)
-        value = jnp.concatenate([value[:half_rows], value[half_rows:] + landed(("q", dz))], 0)
-        r_send(("y", dz), keep(dz, 1, 0, value), dy=1)
-
-    def finish_side_x(dz):
-        value = core_sum(dz, 0, 1)
-        value = jnp.concatenate([value[:half_rows] + landed(("p", dz)), value[half_rows:]], 0)
-        r_send(("x", dz), keep(dz, 0, 1, value), dx=1)
-
-    final = []
-
-    def z_copy(slot, source, target_z):
+        r_send(("p", dz), keep(dz, 1, 1, 0, core_sum(dz, 1, 1, 0)), dy=1)
+        r_send(("q", dz), keep(dz, 1, 1, 1, core_sum(dz, 1, 1, 1)), dx=1)
+
+    def side_copy(side, over, half, source, target_z):
+        slot = side * 4 + over * 2 + half
         return pltpu.make_async_remote_copy(
             src_ref=source,
-            dst_ref=ref["line_parts"].at[slot],
+            dst_ref=ref["sp"].at[slot],
             send_sem=ref["send"].at[0],
-            recv_sem=ref["line_done"].at[slot],
+            recv_sem=ref["sd"].at[slot],
             device_id=device_of(dims, (target_z,) + me[1:]),
             device_id_type=MESH,
         )
 
-    def finish_own(dz):
-        value = core_sum(dz, 0, 0) + landed(("x", dz)) + landed(("y", dz))
+    def side_send(over, half, source):
+        side = jnp.where(zs[1] > me[0], 0, 1)
+        copy = side_copy(side, over, half, source, zs[1])
+        copy.start()
+        sent.append(copy)
+
+    def with_sides(over, half, value):
+        ref["ss"][...] = value
+        for side, source in enumerate((me[0] - 1, me[0] + 1)):
+            there = (source >= 0) & (source < z_count)
+            there &= line_order(source, z_count)[1] == me[0]
+
+            @pl.when(there)
+            def _():
+                at = ref["sp"].at[side * 4 + over * 2 + half]
+                side_copy(side, over, half, at, me[0]).wait_recv()
+                ref["ss"][...] += at[...].astype(jnp.float32)
+
+        return ref["ss"][...]
+
+    def finish_side_y(dz, half):
+        value = core_sum(dz, 1, 0, half)
+        if half:
+            value += landed(("q", dz))
+        if dz == 0 and SIDE_OVER_Z[1]:
+            value = with_sides(1, half, value)
+        at = keep(dz, 1, 0, half, value)
+        if dz == 1 and SIDE_OVER_Z[1]:
+            side_send(1, half, at)
+        else:
+            r_send(("y", dz, half), at, dy=1)
+
+    def finish_side_x(dz, half):
+        value = core_sum(dz, 0, 1, half)
+        if not half:
+            value += landed(("p", dz))
+        if dz == 0 and SIDE_OVER_Z[0]:
+            value = with_sides(0, half, value)
+        at = keep(dz, 0, 1, half, value)
+        if dz == 1 and SIDE_OVER_Z[0]:
+            side_send(0, half, at)
+        else:
+            r_send(("x", dz, half), at, dx=1)
+
+    def z_copy(slot, half, source, target_z):
+        return pltpu.make_async_remote_copy(
+            src_ref=source,
+            dst_ref=ref["lp"].at[slot * 2 + half],
+            send_sem=ref["send"].at[0],
+            recv_sem=ref["ld"].at[slot * 2 + half],
+            device_id=device_of(dims, (target_z,) + me[1:]),
+            device_id_type=MESH,
+        )
+
+    def finish_own(dz, half):
+        value = core_sum(dz, 0, 0, half)
+        for over, side in enumerate(("x", "y")):
+            if not (dz == 1 and SIDE_OVER_Z[over]):
+                value += landed((side, dz, half))
         if dz:
             target = zs[dz]
             slot = lax.rem(me[0] - target + z_count, z_count)
-            copy = z_copy(slot, keep(dz, 0, 0, value), target)
+            copy = z_copy(slot, half, keep(dz, 0, 0, half, value), target)
             copy.start()
             sent.append(copy)
         else:
-            final.append(value)
-
-    def z_landed(turn):
+            ref["os"][half] = value
+
+    def z_landed(turn, half):
         slot = lax.rem(zs[turn] - me[0] + z_count, z_count)
-        at = ref["line_parts"].at[slot]
-        z_copy(slot, at, me[0]).wait_recv()
+        at = ref["lp"].at[slot * 2 + half]
+        z_copy(slot, half, at, me[0]).wait_recv()
         return at[...].astype(jnp.float32)
 
     actions = {
@@ -787,10 +875,11 @@
             actions[entry[0]](*entry[1:])
         else:
             take(*entry)
-    total = final[0]
-    for turn in range(1, z_count):
-        total = total + z_landed(turn)
-    ref["out"][...] = total.astype(jnp.bfloat16)
+    for half in range(2):
+        total = ref["os"][half]
+        for turn in range(1, z_count):
+            total = total + z_landed(turn, half)
+        ref["out"][pl.ds(half * half_rows, half_rows), :] = total.astype(jnp.bfloat16)
     for there, copy in line_sent:
         pl.when(there)(copy.wait_send)
     for copy in sent:
@@ -857,11 +946,16 @@
         "mixes": pltpu.VMEM((sizes["mix"], mix_rows, model_width), bf16),
         "sums": pltpu.VMEM((dims[0] * 4, rows, width), bf16),
         "mix_sum": pltpu.VMEM((mix_rows, model_width), bf16),
-        "line_parts": pltpu.VMEM((dims[0], rows, width), bf16),
-        "line_done": pltpu.SemaphoreType.DMA((dims[0],)),
-        "line_recv": pltpu.SemaphoreType.DMA((len(line_keys(dims)),)),
+        "lp": pltpu.VMEM((2 * dims[0], rows // 2, width), bf16),
+        "sp": pltpu.VMEM((8, rows // 2, width), bf16),
+        "ss": pltpu.VMEM((rows // 2, width), jnp.float32),
+        "sd": pltpu.SemaphoreType.DMA((8,)),
+        "os": pltpu.VMEM((2, rows // 2, width), jnp.float32),
+        "ld": pltpu.SemaphoreType.DMA((2 * dims[0],)),
+        "lr": pltpu.SemaphoreType.DMA((len(line_keys(dims)),)),
         "load_sem": pltpu.SemaphoreType.DMA((len(LOADS),)),
         "send": pltpu.SemaphoreType.DMA((1,)),
+        "pair_recv": pltpu.SemaphoreType.DMA((len(pair_keys(dims)),)),
         "g_recv": pltpu.SemaphoreType.DMA((len(gather_keys(dims)),)),
         "r_recv": pltpu.SemaphoreType.DMA((len(reduce_keys(dims)),)),
     }

time: 52.6 us -> 52.3 us (level)
  no operation moved by 1% of the time
where the time goes in v3:
time: 52.3 us; the launch traced here: 52.2 us
  Pallas kernels  50.2 us (96%)
  local copies, waits for them, and re-layouts  1.31 us (3%)
  between operations  0.65 us (1%)
    pallas_call x1, Pallas kernels, per_device_fused(): pl.pallas_call(functools.partial(layer_kernel, dims, names), out_shape=[p...  50.2 us
    unnamed x2, local copies, waits for them, and re-layouts  1.31 us

profile of v3, /device:TPU:0, one launch (start us, length us, event | category | flops | bytes accessed | tf_op | source)
XLA Modules:
  0.0 52.2 jit_solution(13145031289719429980)
XLA Ops:
  0.6 50.2 %shard_map.203 = (bf16[32,2048]{1,0:T(8,128)(2,1)S(1)}, bf16[128,512]{1,0:T(8,128)(2,1)S(1)}) custom-call(bf16[128,512]{1,0:T(8,128)(2,1)} %refs_0_.1, f32[512]{0:T(512)} %refs_1_.1, bf16[32,128]{1,0:T(8,128)(2,1)} %bitcast.3, f32[32,1024]{1,0:T(8,128)} %constant.2.clone.refs_3_, s32[4,128]{1,0:T(4,128)} %bitcast.4, f32[4,128]{1,0:T(4,128)} %bitcast.5, ...), custom_call_target="tpu_custom_call" | custom-call | tf_op jit(solution)/shard_map/pallas_call | solution.py:964
  50.9 0.7 %copy.24 = bf16[32,2048]{1,0:T(8,128)(2,1)} copy(bf16[32,2048]{1,0:T(8,128)(2,1)S(1)} %get-tuple-element.2) | data formatting | bytes 262144
  51.5 0.7 %copy.25 = bf16[128,512]{1,0:T(8,128)(2,1)} copy(bf16[128,512]{1,0:T(8,128)(2,1)S(1)} %get-tuple-element.3) | data formatting | bytes 262144
